TPU v7x, 128 devices: a whole 4x4x4 slice. The times are simulated.
128 devices in a mesh: rep: 2 (over z_hi), fs: 32 (over z_lo, y, x), tp: 2 (over core).
Axes of the slice: x: 4, y: 4, z: 4 (z_hi: 2, z_lo: 2; z = z_hi * 2 + z_lo), core: 2. Of those that a mesh axis runs over, the one named last changes fastest.
Arguments:
- stream: bfloat16 [64, 512, 2048], P(('rep', 'fs'), None, 'tp'), may hold values from -60 to 60
- pre_gain_mix: float32 [2048], P('tp'), may hold values from 0.1 to 1.9
- value_weight: bfloat16 [2048, 2048], P('fs', 'tp'), may hold values from -0.125 to 0.125
- gate_weight: bfloat16 [2048, 2048], P('fs', 'tp'), may hold values from -0.125 to 0.125
- mix_kernel: bfloat16 [31, 2048], P(None, 'tp'), may hold values from -2 to 2
- mix_bias: float32 [2048], P('tp'), may hold values from -2 to 8
- chan_gain: float32 [2048], P('tp'), may hold values from 0.1 to 1.9
- proj_weight: bfloat16 [2048, 2048], P('fs', 'tp'), may hold values from -2 to 2
- post_gain_mix: float32 [2048], P('tp'), may hold values from 0.1 to 1.9
- pre_gain_ffn: float32 [2048], P('tp'), may hold values from 0.1 to 1.9
- up_gate_weight: bfloat16 [2048, 2816], P('fs', 'tp'), may hold values from -0.125 to 0.125
- up_value_weight: bfloat16 [2048, 2816], P('fs', 'tp'), may hold values from -0.125 to 0.125
- gate_kernel: bfloat16 [3, 2816], P(None, 'tp'), may hold values from -2.5 to 2.5
- value_kernel: bfloat16 [3, 2816], P(None, 'tp'), may hold values from -2.5 to 2.5
- down_weight: bfloat16 [2048, 2816], P('fs', 'tp'), may hold values from -2 to 2
- post_gain_ffn: float32 [2048], P('tp'), may hold values from 0.1 to 1.9
Outputs:
- out_stream: bfloat16 [64, 512, 2048], P(('rep', 'fs'), None, 'tp')
All inputs are finite; a program needn't handle non-finite values.
Results may differ from a plain program's by a relative error of at most 0.014.
Values may be sent and summed in bfloat16 or wider, within the bound.
A program may use at most 128 MiB of HBM per device.

v0:
```python
import jax
import jax.numpy as jnp
from jax import lax
from jax.sharding import PartitionSpec as P

EPS = 1e-06


def over_pieces(x, axis):
    return lax.all_gather(x, axis).sum(0)


def laid_out(tiles, dim):
    lengths = list(tiles.shape[1:])
    lengths[dim] *= tiles.shape[0]
    return jnp.moveaxis(tiles, 0, dim).reshape(lengths)


def from_everyone(x, axis):
    copies = jnp.broadcast_to(x, (lax.axis_size(axis), *x.shape))
    return lax.all_to_all(copies, axis, split_axis=0, concat_axis=0, tiled=True)


def collect(x, axis, dim):
    return laid_out(from_everyone(x, axis), dim)


def in_blocks(x, dim, peers):
    lengths = x.shape
    tiles = x.reshape(*lengths[:dim], peers, lengths[dim] // peers, *lengths[dim + 1 :])
    return jnp.moveaxis(tiles, dim, 0)


def sent_and_summed(x, axis, dim):
    tiles = in_blocks(x, dim, lax.axis_size(axis))
    arrived = lax.all_to_all(tiles, axis, split_axis=0, concat_axis=0, tiled=True)
    return arrived.astype(jnp.float32).sum(axis=0)


def sent_together(arrays, axis, dim, along):
    widths = [a.shape[along] for a in arrays]
    both = jnp.concatenate(arrays, axis=along)
    result = lax.all_gather(both, axis, axis=dim, tiled=True)
    return tuple(jnp.split(result, [sum(widths[:k]) for k in range(1, len(widths))], axis=along))


def square_total(values32):
    return over_pieces(jnp.sum(values32 * values32, axis=1), "tp")


def rms_apply(values32, gain_vector):
    row_width = values32.shape[1] * lax.axis_size("tp")
    inverse_rms = lax.rsqrt(square_total(values32) / row_width + EPS)
    return values32 * inverse_rms[:, None] * gain_vector


def gather_rows(normed):
    return collect(normed, "tp", 1)


def column_total(partial_terms):
    return sent_and_summed(partial_terms.astype(jnp.bfloat16), "tp", 1)


def causal_conv(sequence, kernel):
    taps = kernel.shape[0]
    length = sequence.shape[0]
    padded = jnp.pad(sequence.astype(jnp.float32), ((taps - 1, 0), (0, 0)))
    running = jnp.zeros(sequence.shape, jnp.float32)
    for offset in range(taps):
        running = running + kernel[offset].astype(jnp.float32) * padded[offset : offset + length]
    return running


def contract(activated, weight_rows):
    return lax.dot_general(
        activated, weight_rows, (((1,), (1,)), ((), ())), preferred_element_type=jnp.float32
    )


def per_device(
    stream,
    pre_gain_mix,
    value_weight,
    gate_weight,
    mix_kernel,
    mix_bias,
    chan_gain,
    proj_weight,
    post_gain_mix,
    pre_gain_ffn,
    up_gate_weight,
    up_value_weight,
    gate_kernel,
    value_kernel,
    down_weight,
    post_gain_ffn,
):
    sequence = stream[0]
    normed = rms_apply(sequence.astype(jnp.float32), pre_gain_mix).astype(jnp.bfloat16)
    whole_rows = gather_rows(normed)
    whole_value, whole_gate, whole_proj = sent_together(
        (value_weight, gate_weight, proj_weight), "fs", 0, 1
    )
    value_part = jnp.dot(whole_rows, whole_value, preferred_element_type=jnp.float32)
    gate_part = jnp.dot(whole_rows, whole_gate, preferred_element_type=jnp.float32)
    glu = (value_part * jax.nn.sigmoid(gate_part)).astype(jnp.bfloat16)
    convolved = causal_conv(glu, mix_kernel) + mix_bias
    row_width = convolved.shape[1] * lax.axis_size("tp")
    chan_mean = over_pieces(jnp.sum(convolved, axis=1), "tp") / row_width
    centred = convolved - chan_mean[:, None]
    chan_var = square_total(centred) / row_width
    activated = jax.nn.silu(centred * lax.rsqrt(chan_var + EPS)[:, None] * chan_gain).astype(
        jnp.bfloat16
    )
    partial_terms = contract(activated, whole_proj)
    mixed = column_total(partial_terms).astype(jnp.bfloat16)
    middle = (
        sequence.astype(jnp.float32) + rms_apply(mixed.astype(jnp.float32), post_gain_mix)
    ).astype(jnp.bfloat16)
    normed_ffn = rms_apply(middle.astype(jnp.float32), pre_gain_ffn).astype(jnp.bfloat16)
    whole_ffn_rows = gather_rows(normed_ffn)
    whole_up_gate, whole_up_value, whole_down = sent_together(
        (up_gate_weight, up_value_weight, down_weight), "fs", 0, 1
    )
    gate_sums = jnp.dot(whole_ffn_rows, whole_up_gate, preferred_element_type=jnp.float32)
    value_sums = jnp.dot(whole_ffn_rows, whole_up_value, preferred_element_type=jnp.float32)
    up_gate = gate_sums.astype(jnp.bfloat16)
    up_value = value_sums.astype(jnp.bfloat16)
    hidden = (
        jax.nn.silu(causal_conv(up_gate, gate_kernel)) * causal_conv(up_value, value_kernel)
    ).astype(jnp.bfloat16)
    ffn_terms = contract(hidden, whole_down)
    ffn_out = column_total(ffn_terms).astype(jnp.bfloat16)
    result = (
        middle.astype(jnp.float32) + rms_apply(ffn_out.astype(jnp.float32), post_gain_ffn)
    ).astype(jnp.bfloat16)
    return result[None]


def solution(mesh):
    placed = (
        P(("rep", "fs"), None, "tp"),
        P("tp"),
        P("fs", "tp"),
        P("fs", "tp"),
        P(None, "tp"),
        P("tp"),
        P("tp"),
        P("fs", "tp"),
        P("tp"),
        P("tp"),
        P("fs", "tp"),
        P("fs", "tp"),
        P(None, "tp"),
        P(None, "tp"),
        P("fs", "tp"),
        P("tp"),
    )
    return jax.shard_map(
        per_device,
        mesh=mesh,
        in_specs=placed,
        out_specs=P(("rep", "fs"), None, "tp"),
        check_vma=False,
    )
```

profile of v0, /device:TPU:1, one launch (start us, length us, event | category | flops | bytes accessed | tf_op | source)
XLA Modules:
  0.0 422.9 jit_solution(12970505691127492581)
XLA Ops:
  6.5 1.9 pad_maximum_fusion.1
  8.5 2.0 pad_maximum_fusion
  10.8 2.9 all-gather.6
  16.0 4.2 all-to-all-start
  20.5 2.3 all-to-all-done
  22.7 145.4 %all-gather.15.cloned.1.call-done = bf16[2048,3072]{1,0:T(8,128)(2,1)} async-done(((bf16[64,3072]{1,0:T(8,128)(2,1)}), bf16[2048,3072]{1,0:T(8,128)(2,1)}) %all-gather.15.cloned.1.call-update) | async-done | bytes 12582928 | tf_op jit(solution)/shard_map/all_gather | solution.py:43
  168.2 4.5 %fusion.8 = f32[512,1024]{1,0:T(8,128)S(1)} fusion(bf16[512,2048]{0,1:T(8,128)(2,1)S(1)} %bitcast.103, bf16[2048,3072]{1,0:T(8,128)(2,1)} %all-gather.15.cloned.1.call-done), kind=kOutput, calls=%fused_computation.8 | convolution fusion | flops 2147483648 | bytes 8388608 | tf_op jit(solution)/shard_map/dot_general | solution.py:106
  172.7 4.7 %fusion.85 = f32[512,1024]{1,0:T(8,128)S(1)} fusion(f32[512,1024]{1,0:T(8,128)S(1)} %fusion.8, bf16[512,2048]{0,1:T(8,128)(2,1)S(1)} %bitcast.104, bf16[2048,3072]{1,0:T(8,128)(2,1)} %all-gather.15.cloned.1.call-done), kind=kOutput, calls=%fused_computation.104 | convolution fusion | flops 2150629376 | bytes 10485760 | tf_op jit(solution)/shard_map/dot_general | solution.py:105
  177.5 9.6 %fusion.95 = (f32[512]{0:T(512)S(1)}, f32[512,1024]{1,0:T(8,128)S(1)}) fusion(f32[1024]{0:T(1024)S(1)} %copy-done.9, f32[512,1024]{1,0:T(8,128)S(1)} %fusion.85, f32[1024]{0:T(1024)S(1)} %bitcast.119, f32[1024]{0:T(1024)S(1)} %bitcast.120, f32[1024]{0:T(1024)S(1)} %bitcast.122, f32[1024]{0:T(1024)S(1)} %bitcast.123, f32[1024]{0:T(1024)S(1)} %bitcast.124, ...), kind=kLoop, calls=%fused_computation.157 | loop fusion | flops 33029632 | bytes 4327424 | tf_op jit(solution)/shard_map/reduce_sum | solution.py:110
  187.1 20.6 %all-gather.7 = f32[2,1,512]{2,1,0:T(1,128)S(1)} all-gather(f32[1,1,512]{2,1,0:T(1,128)S(1)} %bitcast.140), channel_id=3, replica_groups=mesh['rep'=2,'fs'=32,'tp'=2] {'tp'}, dimensions={0}, use_global_device_ids=true | all-gather | bytes 6144 | tf_op jit(solution)/shard_map/all_gather | solution.py:10
  210.0 5.0 %fusion.12 = bf16[512,2048]{1,0:T(8,128)(2,1)S(1)} fusion(bf16[2048,3072]{1,0:T(8,128)(2,1)} %all-gather.15.cloned.1.call-done, f32[512,1024]{1,0:T(8,128)S(1)} %get-tuple-element.12, f32[1024]{0:T(1024)S(1)} %copy-done.11, f32[512]{0:T(512)S(1)} %add_rsqrt_fusion.3, f32[512]{0:T(512)S(1)} %broadcast_multiply_fusion), kind=kOutput, calls=%fused_computation.15 | convolution fusion | flops 2152726528 | bytes 8396800 | tf_op jit(solution)/shard_map/dot_general | solution.py:76
  215.2 6.3 %all_to_all.20 = bf16[2,512,1024]{2,1,0:T(8,128)(2,1)} all-to-all(bf16[2,512,1024]{2,1,0:T(8,128)(2,1)S(1)} %bitcast.101), channel_id=1, replica_groups=mesh['rep'=2,'fs'=32,'tp'=2] {'tp'}, dimensions={0} | all-to-all | bytes 4194304 | tf_op jit(solution)/shard_map/all_to_all | solution.py:36
  221.5 2.2 reduce_sum.138
  223.9 2.0 all-gather.9
  226.7 1.8 all-gather.10
  231.8 6.3 %all_to_all.21 = bf16[2,512,1024]{1,2,0:T(8,128)(2,1)} all-to-all(bf16[2,512,1024]{1,2,0:T(8,128)(2,1)S(1)} %broadcast_in_dim.5), channel_id=1, replica_groups=mesh['rep'=2,'fs'=32,'tp'=2] {'tp'}, dimensions={0} | all-to-all | bytes 4194304 | tf_op jit(solution)/shard_map/all_to_all | solution.py:21
  238.0 144.9 %all-gather.17.cloned.1.call-done = bf16[2048,4224]{1,0:T(8,128)(2,1)} async-done(((bf16[64,4224]{1,0:T(8,128)(2,1)}), bf16[2048,4224]{1,0:T(8,128)(2,1)}) %all-gather.17.cloned.1.call-update) | async-done | bytes 17301520 | tf_op jit(solution)/shard_map/all_gather | solution.py:43
  382.9 6.9 %fusion.18 = f32[512,1408]{1,0:T(8,128)S(1)} fusion(bf16[512,2048]{0,1:T(8,128)(2,1)} %bitcast.106, bf16[2048,4224]{1,0:T(8,128)(2,1)} %all-gather.17.cloned.1.call-done), kind=kOutput, calls=%fused_computation.17 | convolution fusion | flops 2954231808 | bytes 10747904 | tf_op jit(solution)/shard_map/dot_general | solution.py:126
  389.9 2.1 copy-done.10
  392.0 3.5 fusion.24
  395.5 7.6 %fusion.27 = bf16[512,2048]{1,0:T(8,128)(2,1)S(1)} fusion(bf16[2048,4224]{1,0:T(8,128)(2,1)} %all-gather.17.cloned.1.call-done, f32[512,1408]{1,0:T(8,128)S(1)} %fusion.24, f32[512,1408]{1,0:T(8,128)S(1)} %fusion.18, f32[1408]{0:T(1024)S(1)} %get-tuple-element.9, f32[1408]{0:T(1024)S(1)} %get-tuple-element.10, f32[1408]{0:T(1024)S(1)} %get-tuple-element.8, ...), kind=kOutput, calls=%fused_computation.20 | convolution fusion | flops 2965372928 | bytes 13665280 | tf_op jit(solution)/shard_map/dot_general | solution.py:76
  403.2 6.8 %all_to_all.22 = bf16[2,512,1024]{2,1,0:T(8,128)(2,1)} all-to-all(bf16[2,512,1024]{2,1,0:T(8,128)(2,1)S(1)} %bitcast.102), channel_id=1, replica_groups=mesh['rep'=2,'fs'=32,'tp'=2] {'tp'}, dimensions={0} | all-to-all | bytes 4194304 | tf_op jit(solution)/shard_map/all_to_all | solution.py:36
  410.0 2.2 reduce_sum.143
  412.5 1.9 all-gather.11
  (57 shorter events, 11.7 us)
Async XLA Ops:
  6.5 4.0 copy-start
  6.5 7.1 %copy-start.6 = (f32[1024]{0:T(1024)S(1)}, f32[1024]{0:T(1024)}, u32[]{:S(2)}) copy-start(f32[1024]{0:T(1024)} %param.17) | copy-start | bytes 12292
  6.5 161.6 %all-gather.15.cloned.1.call-start = ((), (), s32[]{:S(2)}) async-start(), calls=%async_computation.4 | async-start | bytes 12976128 | tf_op jit(solution)/shard_map/all_gather | solution.py:43
  8.5 374.5 %all-gather.17.cloned.1.call-start = ((), (), s32[]{:S(2)}) async-start(), calls=%async_computation.5 | async-start | bytes 17842176 | tf_op jit(solution)/shard_map/all_gather | solution.py:43
  16.0 4.2 %copy-start.4 = (bf16[3,1408]{1,0:T(4,128)(2,1)S(1)}, bf16[3,1408]{1,0:T(4,128)(2,1)}, u32[]{:S(2)}) copy-start(bf16[3,1408]{1,0:T(4,128)(2,1)} %param.29) | copy-start | bytes 25348
  16.0 4.2 %copy-start.5 = (bf16[3,1408]{1,0:T(4,128)(2,1)S(1)}, bf16[3,1408]{1,0:T(4,128)(2,1)}, u32[]{:S(2)}) copy-start(bf16[3,1408]{1,0:T(4,128)(2,1)} %param.28) | copy-start | bytes 25348
  16.0 4.3 %copy-start.2 = (bf16[31,1024]{1,0:T(8,128)(2,1)S(1)}, bf16[31,1024]{1,0:T(8,128)(2,1)}, u32[]{:S(2)}) copy-start(bf16[31,1024]{1,0:T(8,128)(2,1)} %param.20) | copy-start | bytes 190468
  16.0 6.7 %all-to-all-start = ((bf16[2,512,1024]{1,2,0:T(8,128)(2,1)}), bf16[2,512,1024]{1,2,0:T(8,128)(2,1)S(1)}, u32[]{:S(2)}, u32[]{:S(2)}) async-start(bf16[2,512,1024]{1,2,0:T(8,128)(2,1)} %broadcast_in_dim.4), calls=%async_computation | async-start | bytes 4194304 | tf_op jit(solution)/shard_map/all_to_all | solution.py:21
  172.7 4.8 %copy-start.9 = (f32[1024]{0:T(1024)S(1)}, f32[1024]{0:T(1024)}, u32[]{:S(2)}) copy-start(f32[1024]{0:T(1024)} %param.21) | copy-start | bytes 12292
  187.1 22.9 %copy-start.11 = (f32[1024]{0:T(1024)S(1)}, f32[1024]{0:T(1024)}, u32[]{:S(2)}) copy-start(f32[1024]{0:T(1024)} %param.22) | copy-start | bytes 12292
  221.5 4.6 %copy-start.3 = (f32[1024]{0:T(1024)S(1)}, f32[1024]{0:T(1024)}, u32[]{:S(2)}) copy-start(f32[1024]{0:T(1024)} %param.24) | copy-start | bytes 12292
  223.7 4.9 %copy-start.7 = (f32[1024]{0:T(1024)S(1)}, f32[1024]{0:T(1024)}, u32[]{:S(2)}) copy-start(f32[1024]{0:T(1024)} %param.25) | copy-start | bytes 12292
  382.9 7.0 %copy-start.1 = (bf16[2,512,1024]{1,2,0:T(8,128)(2,1)S(1)}, bf16[2,512,1024]{1,2,0:T(8,128)(2,1)}, u32[]{:S(2)}) copy-start(bf16[2,512,1024]{1,2,0:T(8,128)(2,1)} %all_to_all.21) | copy-start | bytes 6291460
  382.9 9.1 %copy-start.10 = (bf16[2048,4224]{1,0:T(8,128)(2,1)S(1)}, bf16[2048,4224]{1,0:T(8,128)(2,1)}, u32[]{:S(2)}) copy-start(bf16[2048,4224]{1,0:T(8,128)(2,1)} %all-gather.17.cloned.1.call-done) | copy-start | bytes 51904516
  410.0 4.4 %copy-start.8 = (f32[1024]{0:T(1024)S(1)}, f32[1024]{0:T(1024)}, u32[]{:S(2)}) copy-start(f32[1024]{0:T(1024)} %param.31) | copy-start | bytes 12292
Sparse Core Ops, SparseCore 0:
  9.0 159.1 all-gather.14
  169.8 213.0 all-gather.16
where the time goes:
time: 424 us; the launch traced here: 423 us
  waiting for transfers between devices  293 us (69%)
  blocking collectives  50.4 us (12%)
  matrix products  32.2 us (8%)
  other arithmetic  23.6 us (6%)
  between operations  13.6 us (3%)
  local copies, waits for them, and re-layouts  6.15 us (1%)
  starting transfers between devices  4.27 us (1%)
    all_gather x2, waiting for transfers between devices, sent_together(): result = lax.all_gather(both, axis, axis=dim, tiled=True)  290 us
    all_gather x6, blocking collectives, over_pieces(): return lax.all_gather(x, axis).sum(0)  31.1 us
    all_to_all x2, blocking collectives, sent_and_summed(): lax.all_to_all(tiles, axis, split_axis=0, concat_axis=0, tiled=True)  13.1 us
    dot_general x2, matrix products, contract(): lax.dot_general(activated, weight_rows, (((1,), (1,)), ((), ())), preferr...  12.5 us
    reduce_sum x1, other arithmetic, per_device(): chan_mean = over_pieces(jnp.sum(convolved, axis=1), 'tp') / row_width  9.61 us
  transfers between devices with their start and end apart: 3, of which 3 were waited for; matrix products, arithmetic and copies ran while one was open for 8% of the time, Pallas kernels for 0%

commit v1 on v0

v1 whole, which is shorter than its diff:
```python
import functools

import jax
import jax.numpy as jnp
from jax import lax
from jax.experimental import pallas as pl
from jax.experimental.pallas import tpu as pltpu
from jax.sharding import PartitionSpec as P

EPS = 1e-06
MESH = pl.DeviceIdType.MESH
F32, BF16 = jnp.float32, jnp.bfloat16

VARIANTS = ((0, 1), (0, -1), (1, 1), (1, -1))
ZSIGN = (1, -1, -1, 1)

class Place:
    def __init__(s):
        fs = lax.axis_index("fs"); zh = lax.axis_index("rep")
        s.core = lax.axis_index("tp")
        s.x = fs % 4; s.y = (fs // 4) % 4; s.zl = fs // 16
        s.z = zh * 2 + s.zl
    def dev(s, dx=0, dy=0, dz=0):
        x = (s.x + dx + 4) % 4; y = (s.y + dy + 4) % 4; z = (s.z + dz + 4) % 4
        return (z // 2, (z % 2) * 16 + y * 4 + x, s.core)
    def partner(s):
        return (lax.axis_index("rep"), lax.axis_index("fs"), 1 - s.core)

class Unit:
    def __init__(s, place, buf, m, split, cols, lo, ssem, rsem, u):
        s.p, s.buf, s.m = place, buf, m
        s.c1 = pl.ds(lo, split); s.c2 = pl.ds(lo + split, cols - split)
        s.ssem, s.rsem, s.u = ssem, rsem, u
        s.sent = []
    def reg(s, q, kind, content, da, db):
        p = s.p; first = VARIANTS[q][0]
        rows = pl.ds(16 * q, 16)
        cols = s.c1 if kind == 1 else s.c2
        zi = slice(None) if content is None else content
        if da is None:
            b = (( p.y if first == 0 else p.x) + db + 4) % 4
            return s.buf.at[s.m, zi, b, :, rows, cols] if first == 0 else s.buf.at[s.m, zi, :, b, rows, cols]
        a = ((p.x if first == 0 else p.y) + da + 4) % 4
        b = ((p.y if first == 0 else p.x) + db + 4) % 4
        y, x = (b, a) if first == 0 else (a, b)
        return s.buf.at[s.m, zi, y, x, rows, cols]
    def to(s, q, da=0, db=0, dz=0):
        first = VARIANTS[q][0]
        return s.p.dev(da, db, dz) if first == 0 else s.p.dev(db, da, dz)
    def copy(s, q, n, region, dev):
        return pltpu.make_async_remote_copy(src_ref=region, dst_ref=region, send_sem=s.ssem.at[s.u, q, n],
            recv_sem=s.rsem.at[s.u, q, n], device_id=dev, device_id_type=MESH)
    def send(s, q, n, region, dev):
        c = s.copy(q, n, region, dev); c.start(); s.sent.append((q, n, region))
    def wait(s, q, n, region):
        s.copy(q, n, region, s.p.dev()).wait_recv()
    def drain(s):
        for q, n, region in s.sent:
            s.copy(q, n, region, s.p.dev()).wait_send()
    def stage(s, k, q):
        mine, other = s.p.zl, 1 - s.p.zl
        f = VARIANTS[q][1]; z = ZSIGN[q]
        near, far = ((0, 1) if f > 0 else (1, 0))
        R, S, W, T = s.reg, s.send, s.wait, s.to
        if k == 0:
            S(q, 0, R(q, 1, mine, 0, 0), T(q, 1)); S(q, 1, R(q, 1, mine, 0, 0), T(q, -1))
            S(q, 10, R(q, 2, mine, 0, 0), T(q, dz=z))
        elif k == 1:
            W(q, near, R(q, 1, mine, -f, 0)); S(q, 2, R(q, 1, mine, -f, 0), T(q, f))
            W(q, 10, R(q, 2, other, 0, 0))
            S(q, 11, R(q, 2, None, 0, 0), T(q, 1)); S(q, 12, R(q, 2, None, 0, 0), T(q, -1))
        elif k == 2:
            W(q, far, R(q, 1, mine, f, 0)); W(q, 2, R(q, 1, mine, 2, 0))
            S(q, 3, R(q, 1, mine, None, 0), T(q, 0, 1)); S(q, 4, R(q, 1, mine, None, 0), T(q, 0, -1))
            S(q, 6, R(q, 1, mine, None, 0), T(q, dz=z))
            W(q, 11 + near, R(q, 2, None, -f, 0)); S(q, 13, R(q, 2, None, -f, 0), T(q, f))
        elif k == 3:
            W(q, 3 + near, R(q, 1, mine, None, -f)); S(q, 5, R(q, 1, mine, None, -f), T(q, 0, f))
            S(q, 7, R(q, 1, mine, None, -f), T(q, dz=z))
            W(q, 3 + far, R(q, 1, mine, None, f)); S(q, 8, R(q, 1, mine, None, f), T(q, dz=z))
            W(q, 11 + far, R(q, 2, None, f, 0)); W(q, 13, R(q, 2, None, 2, 0))
            S(q, 14, R(q, 2, None, None, 0), T(q, 0, 1)); S(q, 15, R(q, 2, None, None, 0), T(q, 0, -1))
        elif k == 4:
            W(q, 5, R(q, 1, mine, None, 2)); S(q, 9, R(q, 1, mine, None, 2), T(q, dz=z))
            W(q, 14 + near, R(q, 2, None, None, -f)); S(q, 16, R(q, 2, None, None, -f), T(q, 0, f))
        elif k == 5:
            W(q, 14 + far, R(q, 2, None, None, f)); W(q, 16, R(q, 2, None, None, 2))
            W(q, 6, R(q, 1, other, None, 0)); W(q, 7, R(q, 1, other, None, -f))
            W(q, 8, R(q, 1, other, None, f)); W(q, 9, R(q, 1, other, None, 2))

def tick(units, t, order=(5, 4, 3, 2, 1, 0)):
    for k in order:
        if 0 <= t - k < len(units):
            for q in range(4):
                units[t - k].stage(k, q)

def barrier(p):
    sem = pltpu.get_barrier_semaphore()
    ds = [p.dev(1), p.dev(-1), p.dev(0, 1), p.dev(0, -1), p.dev(0, 0, 1), p.dev(0, 0, -1), p.partner()]
    for d in ds:
        pl.semaphore_signal(sem, inc=1, device_id=d, device_id_type=MESH)
    pl.semaphore_wait(sem, len(ds))


UNITS = ((0, 0, 1024, 640), (1, 0, 1024, 640), (2, 0, 1024, 640), (3, 0, 1408, 896), (4, 0, 1408, 896), (5, 0, 1408, 896))
ROWS = 512
HALF = 1024
HID = 1408


def norm_rows(a, b, width):
    total = jnp.sum(a * a, axis=1, keepdims=True) + jnp.sum(b * b, axis=1, keepdims=True)
    return lax.rsqrt(total * (1.0 / width) + EPS)


def kernel(
    stream_in, pre_mix_in, value_in, gate_in, taps_in, bias_in, chan_in, proj_in, post_mix_in, pre_ffn_in,
    up_gate_in, up_value_in, gate_taps_in, value_taps_in, down_in, post_ffn_in,
    out,
    wm, wf, xs, xn, val, glu, act, pm, rm, pf, rf, mid, upg, upv, hid, st, gains, taps_b, taps, gtaps_b, vtaps_b, outb,
    ssem, rsem, lsem, psend, precv, osem,
):
    p = Place()
    core = p.core
    partner = p.partner()

    def trade(n, src, dst):
        return pltpu.make_async_remote_copy(
            src_ref=src, dst_ref=dst, send_sem=psend.at[n], recv_sem=precv.at[n], device_id=partner, device_id_type=MESH
        )

    weights = (value_in, gate_in, proj_in, up_gate_in, up_value_in, down_in)
    loads = [
        pltpu.make_async_copy(w, (wm.at[i] if i < 3 else wf.at[i - 3]).at[p.zl, p.y, p.x], lsem.at[i])
        for i, w in enumerate(weights)
    ]
    vectors = (pre_mix_in, post_mix_in, pre_ffn_in, post_ffn_in, bias_in, chan_in)
    small = [pltpu.make_async_copy(stream_in.at[0], xs.at[core], lsem.at[6])]
    small += [pltpu.make_async_copy(v, gains.at[core, i], lsem.at[7 + i]) for i, v in enumerate(vectors)]
    small += [
        pltpu.make_async_copy(taps_in, taps_b, lsem.at[13]),
        pltpu.make_async_copy(gate_taps_in, gtaps_b, lsem.at[14]),
        pltpu.make_async_copy(value_taps_in, vtaps_b, lsem.at[15]),
    ]
    for c in loads + small:
        c.start()
    barrier(p)
    for c in loads:
        c.wait()
    units = [
        Unit(p, wm if m < 3 else wf, m % 3, split, cols, lo, ssem, rsem, u)
        for u, (m, lo, cols, split) in enumerate(UNITS)
    ]
    step = functools.partial(tick, units)
    step(0)
    for c in small:
        c.wait()
    swap_x = trade(0, xs.at[core], xs.at[core])
    swap_g = trade(1, gains.at[core], gains.at[core])
    swap_x.start()
    swap_g.start()
    step(1)
    trade(0, xs.at[1 - core], xs.at[1 - core]).wait_recv()
    trade(1, gains.at[1 - core], gains.at[1 - core]).wait_recv()

    def first_norm(i, _):
        r = pl.ds(pl.multiple_of(i * 16, 16), 16)
        a, b = xs[0, r, :].astype(F32), xs[1, r, :].astype(F32)
        inv = norm_rows(a, b, 2 * HALF)
        xn[0, r, :] = (a * inv * gains[0, 0]).astype(BF16)
        xn[1, r, :] = (b * inv * gains[1, 0]).astype(BF16)
        return 0

    step(2)
    lax.fori_loop(0, ROWS // 16, first_norm, 0)
    taps[0:31, :] = taps_b[...].astype(F32)
    glu[0:32, :] = jnp.zeros((32, HALF), F32)
    upg[0:8, :] = jnp.zeros((8, HID), F32)
    upv[0:8, :] = jnp.zeros((8, HID), F32)

    def product(buf, m, c):
        w0 = buf[m, 0, :, :, :, c].reshape(HALF, c.size)
        w1 = buf[m, 1, :, :, :, c].reshape(HALF, c.size)
        return jnp.dot(xn[0], w0, preferred_element_type=F32) + jnp.dot(xn[1], w1, preferred_element_type=F32)

    def blocks(width, body):
        def one(i, _):
            body(pl.ds(pl.multiple_of(i * 256, 256), 256))
            return 0

        lax.fori_loop(0, width // 256, one, 0)
        if width % 256:
            body(pl.ds(width // 256 * 256, width % 256))

    step(3)
    step(4)
    step(5)

    def value_block(c):
        val[:, c] = product(wm, 0, c)

    blocks(HALF, value_block)
    step(6)

    def gate_block(c):
        g = product(wm, 1, c)
        glu[32 : 32 + ROWS, c] = (val[:, c] * jax.nn.sigmoid(g)).astype(BF16).astype(F32)

    blocks(HALF, gate_block)

    def conv_block(i, _):
        c = pl.ds(pl.multiple_of((i % 8) * 128, 128), 128)
        t = pl.multiple_of((i // 8) * 64, 64)
        g = glu[pl.ds(t, 96), c]
        total = jnp.broadcast_to(gains[core, 4, :, c], (64, 128))
        for k in range(8):
            part = None
            rows = 72 if k else 64
            for j in range(31):
                if (2 + j) % 8 == k:
                    at = (2 + j) // 8 * 8
                    term = taps[j : j + 1, c] * g[at : at + rows]
                    part = term if part is None else part + term
            total = total + part[k : k + 64]
        val[pl.ds(t, 64), c] = total
        return 0

    lax.fori_loop(0, 64, conv_block, 0)

    def stats_block(i, _):
        r = pl.ds(pl.multiple_of(i * 32, 32), 32)
        v = val[r, :]
        mean = jnp.sum(v, axis=1, keepdims=True) * (1.0 / HALF)
        d = v - mean
        st[core, 0, r, :] = jnp.broadcast_to(mean, (32, 128))
        st[core, 1, r, :] = jnp.broadcast_to(jnp.sum(d * d, axis=1, keepdims=True), (32, 128))
        return 0

    lax.fori_loop(0, ROWS // 32, stats_block, 0)
    swap_s = trade(2, st.at[core], st.at[core])
    swap_s.start()
    step(7)
    trade(2, st.at[1 - core], st.at[1 - core]).wait_recv()

    def act_block(i, _):
        r = pl.ds(pl.multiple_of(i * 32, 32), 32)
        m0, m1 = st[0, 0, r, :][:, :1], st[1, 0, r, :][:, :1]
        gap = m0 - m1
        var = (st[0, 1, r, :][:, :1] + st[1, 1, r, :][:, :1] + gap * gap * (HALF / 2)) * (0.5 / HALF)
        h = (val[r, :] - (m0 + m1) * 0.5) * lax.rsqrt(var + EPS) * gains[core, 5]
        act[r, :] = jax.nn.silu(h).astype(BF16)
        return 0

    lax.fori_loop(0, ROWS // 32, act_block, 0)

    def rows_product(lhs, buf, mine, theirs, base):
        def region(ref, i):
            return ref.at[i // 4, :, pl.ds(pl.multiple_of((i % 4) * 256, 256), 256)]

        def send(i):
            trade(base + i, region(mine, i), region(theirs, i)).start()

        def one(i, _):
            w = buf[2, i // 4, i % 4].reshape(256, lhs.shape[1])
            part = lax.dot_general(lhs[...], w, (((1,), (1,)), ((), ())), preferred_element_type=F32)
            mine[i // 4, :, pl.ds(pl.multiple_of((i % 4) * 256, 256), 256)] = part.astype(BF16)

            @pl.when(i > 0)
            def _():
                send(i - 1)

            return 0

        lax.fori_loop(0, 8, one, 0)
        send(7)

        def arrive(i, _):
            trade(base + i, region(theirs, i), region(theirs, i)).wait_recv()
            return 0

        def leave(i, _):
            trade(base + i, region(mine, i), region(theirs, i)).wait_send()
            return 0

        return lambda: lax.fori_loop(0, 8, arrive, 0), lambda: lax.fori_loop(0, 8, leave, 0)

    mix_arrive, mix_leave = rows_product(act, wm, pm, rm, 3)
    step(8)
    mix_arrive()

    def middle_block(i, _):
        r = pl.ds(pl.multiple_of(i * 16, 16), 16)
        a = (pm[0, r, :].astype(F32) + rm[0, r, :].astype(F32)).astype(BF16).astype(F32)
        b = (pm[1, r, :].astype(F32) + rm[1, r, :].astype(F32)).astype(BF16).astype(F32)
        inv = norm_rows(a, b, 2 * HALF)
        a = (xs[0, r, :].astype(F32) + a * inv * gains[0, 1]).astype(BF16)
        b = (xs[1, r, :].astype(F32) + b * inv * gains[1, 1]).astype(BF16)
        mid[0, r, :] = a
        mid[1, r, :] = b
        a, b = a.astype(F32), b.astype(F32)
        inv = norm_rows(a, b, 2 * HALF)
        xn[0, r, :] = (a * inv * gains[0, 2]).astype(BF16)
        xn[1, r, :] = (b * inv * gains[1, 2]).astype(BF16)
        return 0

    lax.fori_loop(0, ROWS // 16, middle_block, 0)

    def up_block(dst, m, c):
        dst[8 : 8 + ROWS, c] = product(wf, m, c).astype(BF16).astype(F32)

    blocks(HID, functools.partial(up_block, upg, 0))
    step(9)
    blocks(HID, functools.partial(up_block, upv, 1))

    def hidden_block(i, _):
        c = pl.ds(pl.multiple_of((i // 8) * 128, 128), 128)
        t = pl.multiple_of((i % 8) * 64, 64)
        g, v = upg[pl.ds(t, 72), c], upv[pl.ds(t, 72), c]
        kg, kv = gtaps_b[:, c].astype(F32), vtaps_b[:, c].astype(F32)
        gc = kg[0:1] * g[6:70] + kg[1:2] * g[7:71] + kg[2:3] * g[8:72]
        vc = kv[0:1] * v[6:70] + kv[1:2] * v[7:71] + kv[2:3] * v[8:72]
        hid[pl.ds(t, 64), c] = (jax.nn.silu(gc) * vc).astype(BF16)
        return 0

    lax.fori_loop(0, 8 * (HID // 128), hidden_block, 0)
    step(10)
    ffn_arrive, ffn_leave = rows_product(hid, wf, pf, rf, 11)
    ffn_arrive()

    def out_block(i, _):
        r = pl.ds(pl.multiple_of(i * 16, 16), 16)
        a = (pf[core, r, :].astype(F32) + rf[core, r, :].astype(F32)).astype(BF16).astype(F32)
        b = (pf[1 - core, r, :].astype(F32) + rf[1 - core, r, :].astype(F32)).astype(BF16).astype(F32)
        inv = norm_rows(a, b, 2 * HALF)
        outb[r, :] = (mid[core, r, :].astype(F32) + a * inv * gains[core, 3]).astype(BF16)
        return 0

    stores = []
    for k in range(4):
        lax.fori_loop(8 * k, 8 * k + 8, out_block, 0)
        c = pltpu.make_async_copy(outb.at[pl.ds(128 * k, 128)], out.at[0, pl.ds(128 * k, 128)], osem.at[k])
        c.start()
        stores.append(c)
    swap_x.wait_send()
    swap_g.wait_send()
    swap_s.wait_send()
    mix_leave()
    ffn_leave()
    for u in units:
        u.drain()
    for c in stores:
        c.wait()


def per_device(*args):
    arrays = [a.reshape(1, -1) if a.ndim == 1 else a for a in args]
    sems = pltpu.SemaphoreType.DMA
    return pl.pallas_call(
        kernel,
        out_shape=jax.ShapeDtypeStruct((1, ROWS, HALF), BF16),
        in_specs=[pl.BlockSpec(memory_space=pl.ANY)] * len(arrays),
        out_specs=pl.BlockSpec(memory_space=pl.ANY),
        scratch_shapes=[
            pltpu.VMEM((3, 2, 4, 4, 64, HALF), BF16),
            pltpu.VMEM((3, 2, 4, 4, 64, HID), BF16),
            pltpu.VMEM((2, ROWS, HALF), BF16),
            pltpu.VMEM((2, ROWS, HALF), BF16),
            pltpu.VMEM((ROWS, HALF), F32),
            pltpu.VMEM((32 + ROWS, HALF), F32),
            pltpu.VMEM((ROWS, HALF), BF16),
            pltpu.VMEM((2, ROWS, HALF), BF16),
            pltpu.VMEM((2, ROWS, HALF), BF16),
            pltpu.VMEM((2, ROWS, HALF), BF16),
            pltpu.VMEM((2, ROWS, HALF), BF16),
            pltpu.VMEM((2, ROWS, HALF), BF16),
            pltpu.VMEM((8 + ROWS, HID), F32),
            pltpu.VMEM((8 + ROWS, HID), F32),
            pltpu.VMEM((ROWS, HID), BF16),
            pltpu.VMEM((2, 2, ROWS, 128), F32),
            pltpu.VMEM((2, 6, 1, HALF), F32),
            pltpu.VMEM((31, HALF), BF16),
            pltpu.VMEM((32, HALF), F32),
            pltpu.VMEM((3, HID), BF16),
            pltpu.VMEM((3, HID), BF16),
            pltpu.VMEM((ROWS, HALF), BF16),
            sems((len(UNITS), 4, 17)),
            sems((len(UNITS), 4, 17)),
            sems((16,)),
            sems((19,)),
            sems((19,)),
            sems((4,)),
        ],
        compiler_params=pltpu.CompilerParams(collective_id=0, has_side_effects=True, vmem_limit_bytes=67043328),
    )(*arrays)


def solution(mesh):
    rows = P(("rep", "fs"), None, "tp")
    vector, matrix, taps = P("tp"), P("fs", "tp"), P(None, "tp")
    placed = (
        rows, vector, matrix, matrix, taps, vector, vector, matrix, vector, vector,
        matrix, matrix, taps, taps, matrix, vector,
    )
    return jax.shard_map(per_device, mesh=mesh, in_specs=placed, out_specs=rows, check_vma=False)
```

time: 424 us -> 145 us (0.34)
  waiting for transfers between devices: 293 us -> 0 us
  Pallas kernels: 0 us -> 142 us
  blocking collectives: 50.4 us -> 0 us
  matrix products: 32.2 us -> 0 us
  other arithmetic: 23.6 us -> 0 us
  between operations: 13.6 us -> 0.01 us
  starting transfers between devices: 4.27 us -> 0 us
    all_gather x2 -> x0, waiting for transfers between devices: 290 us -> none  [sent_together(): result = lax.all_gather(both, axis, axis=dim, tiled=True)]
    pallas_call x0 -> x1, Pallas kernels: none -> 142 us  [per_device(): pl.pallas_call(kernel, out_shape=jax.ShapeDtypeStruct((1, ROWS, HALF), BF...]
    dot_general x6 -> x0, matrix products: 32.2 us -> none  [the longest x2 12.5 us: contract(): lax.dot_general(activated, weight_rows, (((1,), (1,)), ((), ())), preferr...]
    all_gather x6 -> x0, blocking collectives: 31.1 us -> none  [over_pieces(): return lax.all_gather(x, axis).sum(0)]
    all_to_all x3 -> x0, blocking collectives: 19.3 us -> none  [the longest x2 13.1 us: sent_and_summed(): lax.all_to_all(tiles, axis, split_axis=0, concat_axis=0, tiled=True)]
    reduce_sum x14 -> x0, other arithmetic: 15.9 us -> none  [the longest x1 9.61 us: per_device(): chan_mean = over_pieces(jnp.sum(convolved, axis=1), 'tp') / row_width]
  transfers between devices with their start and end apart: 3 -> 0, of which waited for: 3 -> 0; matrix products, arithmetic and copies ran while one was open for 8% -> 0% of each run, Pallas kernels for 0% -> 0%
where the time goes in v1:
time: 145 us
  Pallas kernels  142 us (98%)
  local copies, waits for them, and re-layouts  2.26 us (2%)
    pallas_call x1, Pallas kernels, per_device(): pl.pallas_call(kernel, out_shape=jax.ShapeDtypeStruct((1, ROWS, HALF), BF...  142 us

profile of v1, /device:TPU:1, one launch (start us, length us, event | category | flops | bytes accessed | tf_op | source)
XLA Modules:
  0.0 144.6 jit_solution(8089518048708113467)
XLA Ops:
  0.0 142.3 %shard_map.154 = bf16[1,512,1024]{2,1,0:T(8,128)(2,1)} custom-call(bf16[1,512,1024]{2,1,0:T(8,128)(2,1)} %stream_in.1, f32[1,1024]{1,0:T(1,128)} %bitcast.6, bf16[64,1024]{1,0:T(8,128)(2,1)} %value_in.1, bf16[64,1024]{1,0:T(8,128)(2,1)} %gate_in.1, bf16[31,1024]{1,0:T(8,128)(2,1)} %taps_in.1, f32[1,1024]{1,0:T(1,128)} %bitcast.7, f32[1,1024]{1,0:T(1,128)} %bitcast.8, ...), custom_call_target="tpu_custom_call" | custom-call | tf_op jit(solution)/shard_map/pallas_call | solution.py:358
  142.3 2.3 %copy.18 = bf16[1,512,1024]{2,1,0:T(8,128)(2,1)} copy(bf16[1,512,1024]{2,1,0:T(8,128)(2,1)} %shard_map.154) | data formatting | bytes 2097152

commit v2 on v1

v2 whole, which is shorter than its diff:
```python
import functools

import jax
import jax.numpy as jnp
from jax import lax
from jax.experimental import pallas as pl
from jax.experimental.pallas import tpu as pltpu
from jax.sharding import PartitionSpec as P

EPS = 1e-06
MESH = pl.DeviceIdType.MESH
F32, BF16 = jnp.float32, jnp.bfloat16

class Place:
    def __init__(s):
        fs = lax.axis_index("fs"); zh = lax.axis_index("rep")
        s.core = lax.axis_index("tp")
        s.x = fs % 4; s.y = (fs // 4) % 4; s.zl = fs // 16
        s.z = zh * 2 + s.zl
    def dev(s, dx=0, dy=0, dz=0):
        x = (s.x + dx + 4) % 4; y = (s.y + dy + 4) % 4; z = (s.z + dz + 4) % 4
        return (z // 2, (z % 2) * 16 + y * 4 + x, s.core)
    def partner(s):
        return (lax.axis_index("rep"), lax.axis_index("fs"), 1 - s.core)

class Unit:
    WAITS = (6, 7)

    def __init__(s, place, buf, m, lo, cols, split, ssem, rsem, u, base):
        s.p, s.buf, s.m = place, buf, m
        s.c1, s.c2, s.all_columns = pl.ds(lo, split), pl.ds(lo + split, cols - split), pl.ds(lo, cols)
        s.ssem, s.rsem = ssem.at[u], rsem
        s.base = (base, base + (13 if split else 0))

    @staticmethod
    def semaphores(cols, split):
        return (13 if split else 0) + (14 if split < cols else 0)

    def region(s, g, kind, part, content, da, db):
        rows = pl.ds(32 * g + 16 * max(part, 0), 32 if part < 0 else 16)
        cols = s.c1 if kind == 1 else s.c2
        z = slice(None) if content is None else content
        first, second = (s.p.x, s.p.y) if g == 0 else (s.p.y, s.p.x)
        a = slice(None) if da is None else (first + da + 4) % 4
        b = (second + db + 4) % 4
        y, x = (b, a) if g == 0 else (a, b)
        return s.buf.at[s.m, z, y, x, rows, cols]

    def copy(s, n, region, dev):
        return pltpu.make_async_remote_copy(
            src_ref=region, dst_ref=region, send_sem=s.ssem, recv_sem=s.rsem.at[n], device_id=dev, device_id_type=MESH
        )

    def drain(s):
        whole = s.buf.reshape(3, 32, *s.buf.shape[4:]).at[s.m, pl.ds(0, 31), :, s.all_columns]
        s.copy(0, whole, s.p.dev()).wait_send()

    def stage(s, kind, k, g):
        if (s.c1 if kind == 1 else s.c2).size == 0:
            return
        mine, other, R = s.p.zl, 1 - s.p.zl, functools.partial(s.region, g, kind)
        sem = s.base[kind - 1] + g * s.WAITS[kind - 1]
        up = 1 - 2 * g
        signs = ((0, 1), (1, -1))

        def send(n, region, da=0, db=0, dz=0):
            s.copy(sem + n, region, s.p.dev(da, db, dz) if g == 0 else s.p.dev(db, da, dz)).start()

        def to_z(region):
            s.copy(s.base[0] + 12, region, s.p.dev(0, 0, up)).start()

        def wait(n, region):
            s.copy(sem + n, region, s.p.dev()).wait_recv()

        if (kind, k) == (1, 0):
            for i, d in signs:
                send(i, R(-1, mine, 0, 0), d)
        elif (kind, k) == (1, 1):
            for i, d in signs:
                wait(i, R(-1, mine, -d, 0))
                send(2, R(i, mine, -d, 0), d)
        elif (kind, k) == (1, 2):
            wait(2, R(-1, mine, 2, 0))
            for i, d in signs:
                send(3 + i, R(-1, mine, None, 0), 0, d)
            to_z(R(-1, mine, None, 0))
        elif (kind, k) == (1, 3):
            for i, d in signs:
                wait(3 + i, R(-1, mine, None, -d))
                send(5, R(i, mine, None, -d), 0, d)
                to_z(R(-1, mine, None, -d))
        elif (kind, k) == (1, 4):
            wait(5, R(-1, mine, None, 2))
            to_z(R(-1, mine, None, 2))
        elif (kind, k) == (1, 5):
            if g == 0:
                wait(12, s.buf.at[s.m, other, :, :, :, s.c1])
        elif (kind, k) == (2, 0):
            send(0, R(-1, mine, 0, 0), 0, 0, up)
        elif (kind, k) == (2, 1):
            wait(0, R(-1, other, 0, 0))
            for i, d in signs:
                send(1 + i, R(-1, None, 0, 0), d)
        elif (kind, k) == (2, 2):
            for i, d in signs:
                wait(1 + i, R(-1, None, -d, 0))
                send(3, R(i, None, -d, 0), d)
        elif (kind, k) == (2, 3):
            wait(3, R(-1, None, 2, 0))
            for i, d in signs:
                send(4 + i, R(-1, None, None, 0), 0, d)
        elif (kind, k) == (2, 4):
            for i, d in signs:
                wait(4 + i, R(-1, None, None, -d))
                send(6, R(i, None, None, -d), 0, d)
        elif (kind, k) == (2, 5):
            wait(6, R(-1, None, None, 2))


def barrier(p):
    sem = pltpu.get_barrier_semaphore()
    ds = [p.dev(1), p.dev(-1), p.dev(0, 1), p.dev(0, -1), p.dev(0, 0, 1), p.dev(0, 0, -1), p.partner()]
    for d in ds:
        pl.semaphore_signal(sem, inc=1, device_id=d, device_id_type=MESH)
    pl.semaphore_wait(sem, len(ds))


UNITS = (
    (0, pl.ds(0, 2), 0, 1024, 512),
    (0, 2, 0, 1024, 896),
    (1, pl.ds(0, 2), 0, 768, 768),
    (1, pl.ds(0, 2), 768, 640, 256),
    (1, 2, 0, 896, 0),
    (1, 2, 896, 512, 384),
)
DOWN = (0, 896, 1408)
SCHEDULE = (
    ("u", 0, 1, 0), ("u", 0, 2, 0), ("start",), ("u", 1, 1, 0), ("u", 1, 2, 0), ("u", 2, 1, 0), ("u", 3, 2, 0),
    ("u", 3, 1, 0), ("u", 4, 2, 0), ("u", 5, 2, 0), ("u", 5, 1, 0), ("u", 0, 1, 1), ("u", 0, 2, 1), ("norm",),
    ("u", 0, 1, 2), ("u", 0, 2, 2), ("u", 1, 1, 1), ("u", 1, 2, 1), ("u", 0, 1, 3), ("u", 0, 2, 3), ("u", 1, 1, 2),
    ("u", 1, 2, 2), ("u", 2, 1, 1), ("u", 0, 1, 4), ("u", 0, 2, 4), ("u", 1, 1, 3), ("u", 1, 2, 3), ("u", 2, 1, 2),
    ("u", 3, 2, 1), ("u", 3, 1, 1), ("u", 0, 1, 5), ("u", 0, 2, 5), ("glu", 0), ("glu", 1), ("u", 1, 1, 4), ("glu", 2),
    ("u", 1, 2, 4), ("glu", 3), ("conv", 0), ("conv", 1), ("conv", 2), ("conv", 3), ("u", 2, 1, 3), ("stats",),
    ("u", 3, 2, 2), ("u", 3, 1, 2), ("u", 4, 2, 1), ("u", 1, 2, 5), ("act",), ("u", 1, 1, 5), ("u", 2, 1, 4),
    ("u", 3, 2, 3), ("proj", 0), ("u", 3, 1, 3), ("proj", 1), ("u", 4, 2, 2), ("u", 5, 1, 1), ("u", 5, 2, 1),
    ("mid", 0), ("mid", 1), ("u", 3, 2, 4), ("u", 3, 1, 4), ("u", 4, 2, 3), ("u", 5, 1, 2), ("u", 5, 2, 2),
    ("u", 3, 2, 5), ("u", 2, 1, 5), ("up", 0), ("up", 1), ("up", 2), ("hid", 0), ("u", 4, 2, 4), ("hid", 1),
    ("u", 5, 1, 3), ("u", 5, 2, 3), ("u", 3, 1, 5), ("up", 3), ("up", 4), ("up", 5), ("hid", 2), ("u", 4, 2, 5),
    ("hid", 3), ("u", 5, 1, 4), ("u", 5, 2, 4), ("down", 0), ("u", 5, 1, 5), ("u", 5, 2, 5), ("down", 1),
)
ROWS = 512
HALF = 1024
HID = 1408


def norm_rows(a, b, width):
    total = jnp.sum(a * a, axis=1, keepdims=True) + jnp.sum(b * b, axis=1, keepdims=True)
    return lax.rsqrt(total * (1.0 / width) + EPS)


def kernel(
    stream_in, pre_mix_in, value_in, gate_in, taps_in, bias_in, chan_in, proj_in, post_mix_in, pre_ffn_in,
    up_gate_in, up_value_in, gate_taps_in, value_taps_in, down_in, post_ffn_in,
    out,
    wm, wf, xs, xn, val, glu, act, pm, rm, pf, rf, mid, upg, upv, hid, st, gains, taps_b, taps, gtaps_b, vtaps_b,
    ssem, rsem, lsem, psend, precv,
):
    p = Place()
    core = p.core
    partner = p.partner()

    def trade(n, src, dst):
        return pltpu.make_async_remote_copy(
            src_ref=src, dst_ref=dst, send_sem=psend.at[n], recv_sem=precv.at[n], device_id=partner, device_id_type=MESH
        )

    def load(src, dst, n):
        return pltpu.make_async_copy(src, dst, lsem.at[n])

    for i, w in enumerate((value_in, gate_in, proj_in)):
        load(w, wm.at[i, p.zl, p.y, p.x], 0).start()
    for i, w in enumerate((up_gate_in, up_value_in, down_in)):
        load(w, wf.at[i, p.zl, p.y, p.x], 1).start()
    for i, v in enumerate((pre_mix_in, post_mix_in, pre_ffn_in, post_ffn_in, bias_in, chan_in)):
        load(v, gains.at[core, i], 2).start()
    small = [load(stream_in.at[0], xs.at[core], 3), load(taps_in, taps_b, 4), load(gate_taps_in, gtaps_b, 5), load(value_taps_in, vtaps_b, 6)]
    for c in small:
        c.start()
    barrier(p)
    for n, whole in enumerate((wm.at[:, p.zl, p.y, p.x], wf.at[:, p.zl, p.y, p.x])):
        load(whole, whole, n).wait()
    units, base = [], 0
    for u, (ffn, m, lo, cols, split) in enumerate(UNITS):
        units.append(Unit(p, wf if ffn else wm, m, lo, cols, split, ssem, rsem, u, base))
        base += Unit.semaphores(cols, split)
    swap_x = trade(0, xs.at[core], xs.at[core])
    swap_g = trade(1, gains.at[core], gains.at[core])

    def start():
        load(gains.at[core], gains.at[core], 2).wait()
        for c in small:
            c.wait()
        swap_x.start()
        swap_g.start()
        taps[0:31, :] = taps_b[...].astype(F32)
        glu[0:32, :] = jnp.zeros((32, HALF), F32)
        upg[0:8, :] = jnp.zeros((8, HID), F32)
        upv[0:8, :] = jnp.zeros((8, HID), F32)

    def first_norm(i, _):
        r = pl.ds(pl.multiple_of(i * 16, 16), 16)
        a, b = xs[0, r, :].astype(F32), xs[1, r, :].astype(F32)
        inv = norm_rows(a, b, 2 * HALF)
        xn[0, r, :] = (a * inv * gains[0, 0]).astype(BF16)
        xn[1, r, :] = (b * inv * gains[1, 0]).astype(BF16)
        return 0

    def norm():
        trade(0, xs.at[1 - core], xs.at[1 - core]).wait_recv()
        trade(1, gains.at[1 - core], gains.at[1 - core]).wait_recv()
        lax.fori_loop(0, ROWS // 16, first_norm, 0, unroll=2)

    def product(buf, m, c):
        w0 = buf[m, 0, :, :, :, c].reshape(HALF, c.size)
        w1 = buf[m, 1, :, :, :, c].reshape(HALF, c.size)
        return jnp.dot(xn[0], w0, preferred_element_type=F32) + jnp.dot(xn[1], w1, preferred_element_type=F32)

    def blocks(first, width, body):
        def one(i, _):
            body(pl.ds(pl.multiple_of(first + i * 256, 256), 256))
            return 0

        lax.fori_loop(0, width // 256, one, 0)
        if width % 256:
            body(pl.ds(first + width // 256 * 256, width % 256))

    def glu_block(c):
        v, g = product(wm, 0, c), product(wm, 1, c)
        glu[32 : 32 + ROWS, c] = (v * jax.nn.sigmoid(g)).astype(BF16).astype(F32)

    def conv_block(i, _):
        c = pl.ds(pl.multiple_of((i // 8) * 128, 128), 128)
        t = pl.multiple_of((i % 8) * 64, 64)
        g = glu[pl.ds(t, 96), c]
        total = jnp.broadcast_to(gains[core, 4, :, c], (64, 128))
        for k in range(8):
            part = None
            rows = 72 if k else 64
            for j in range(31):
                if (2 + j) % 8 == k:
                    at = (2 + j) // 8 * 8
                    term = taps[j : j + 1, c] * g[at : at + rows]
                    part = term if part is None else part + term
            total = total + part[k : k + 64]
        val[pl.ds(t, 64), c] = total
        return 0

    def stats_block(i, _):
        r = pl.ds(pl.multiple_of(i * 32, 32), 32)
        v = val[r, :]
        mean = jnp.sum(v, axis=1, keepdims=True) * (1.0 / HALF)
        d = v - mean
        st[core, 0, r, :] = jnp.broadcast_to(mean, (32, 128))
        st[core, 1, r, :] = jnp.broadcast_to(jnp.sum(d * d, axis=1, keepdims=True), (32, 128))
        return 0

    def act_block(i, _):
        r = pl.ds(pl.multiple_of(i * 32, 32), 32)
        m0, m1 = st[0, 0, r, :][:, :1], st[1, 0, r, :][:, :1]
        gap = m0 - m1
        var = (st[0, 1, r, :][:, :1] + st[1, 1, r, :][:, :1] + gap * gap * (HALF / 2)) * (0.5 / HALF)
        h = (val[r, :] - (m0 + m1) * 0.5) * lax.rsqrt(var + EPS) * gains[core, 5]
        act[r, :] = jax.nn.silu(h).astype(BF16)
        return 0

    def region(ref, i):
        return ref.at[i // 2, :, pl.ds(512 * (i % 2), 512)]

    def rows_product(lhs, buf, part, total, mine, theirs, base, lo, hi):
        def send(i):
            trade(base, region(mine, i), region(theirs, i)).start()

        for i in range(lo, hi):
            h, n = i // 2, i % 2
            w = buf[2, h, 2 * n : 2 * n + 2, :, :, part].reshape(512, part.size)
            c = pl.ds(512 * n, 512)
            term = lax.dot_general(lhs[:, part], w, (((1,), (1,)), ((), ())), preferred_element_type=F32)
            if mine is None:
                total[h][0:ROWS, c] = term
                continue
            mine[h, :, c] = (term if total is None else total[h][0:ROWS, c] + term).astype(BF16)
            if i > lo:
                send(i - 1)
        if mine is not None:
            send(hi - 1)

    def middle_block(i, _):
        r = pl.ds(pl.multiple_of(i * 16, 16), 16)
        a = (pm[0, r, :].astype(F32) + rm[0, r, :].astype(F32)).astype(BF16).astype(F32)
        b = (pm[1, r, :].astype(F32) + rm[1, r, :].astype(F32)).astype(BF16).astype(F32)
        inv = norm_rows(a, b, 2 * HALF)
        a = (xs[0, r, :].astype(F32) + a * inv * gains[0, 1]).astype(BF16)
        b = (xs[1, r, :].astype(F32) + b * inv * gains[1, 1]).astype(BF16)
        mid[0, r, :] = a
        mid[1, r, :] = b
        a, b = a.astype(F32), b.astype(F32)
        inv = norm_rows(a, b, 2 * HALF)
        xn[0, r, :] = (a * inv * gains[0, 2]).astype(BF16)
        xn[1, r, :] = (b * inv * gains[1, 2]).astype(BF16)
        return 0

    def up_block(c):
        g, v = product(wf, 0, c), product(wf, 1, c)
        upg[8 : 8 + ROWS, c] = g.astype(BF16).astype(F32)
        upv[8 : 8 + ROWS, c] = v.astype(BF16).astype(F32)

    def hidden_block(i, _):
        c = pl.ds(pl.multiple_of((i // 8) * 128, 128), 128)
        t = pl.multiple_of((i % 8) * 64, 64)
        g, v = upg[pl.ds(t, 72), c], upv[pl.ds(t, 72), c]
        kg, kv = gtaps_b[:, c].astype(F32), vtaps_b[:, c].astype(F32)
        gc = kg[0:1] * g[6:70] + kg[1:2] * g[7:71] + kg[2:3] * g[8:72]
        vc = kv[0:1] * v[6:70] + kv[1:2] * v[7:71] + kv[2:3] * v[8:72]
        hid[pl.ds(t, 64), c] = (jax.nn.silu(gc) * vc).astype(BF16)
        return 0

    swap_s = trade(2, st.at[core], st.at[core])

    def stats():
        lax.fori_loop(0, ROWS // 32, stats_block, 0, unroll=2)
        swap_s.start()

    def activate():
        trade(2, st.at[1 - core], st.at[1 - core]).wait_recv()
        lax.fori_loop(0, ROWS // 32, act_block, 0, unroll=2)

    def project(i):
        rows_product(act, wm, pl.ds(0, HALF), None, pm, rm, 3, 2 * i, 2 * i + 2)

    def middle(i):
        if i == 0:
            trade(3, rm, rm).wait_recv()
        n = ROWS // 32
        lax.fori_loop(n * i, n * i + n, middle_block, 0, unroll=2)

    def glu_piece(i):
        glu_block(pl.ds(256 * i, 256))

    def conv(i):
        lax.fori_loop(16 * i, 16 * i + 16, conv_block, 0)

    def up(i):
        up_block(pl.ds(256 * i, min(256, HID - 256 * i)))

    def hidden(i):
        lo, hi = ((0, 24), (24, 48), (48, 68), (68, 88))[i]
        lax.fori_loop(lo, hi, hidden_block, 0)

    def down(i):
        part = pl.ds(DOWN[i], DOWN[i + 1] - DOWN[i])
        last = i + 2 == len(DOWN)
        rows_product(hid, wf, part, (val, glu) if i < 1 < len(DOWN) - 1 or i else None, pf if last else None, rf, 4, 0, 4)

    pieces = dict(
        start=start, norm=norm, glu=glu_piece, conv=conv, stats=stats, act=activate, proj=project, mid=middle, up=up, hid=hidden, down=down
    )
    for name, *numbers in SCHEDULE:
        if name == "u":
            u, kind, k = numbers
            for g in range(2):
                units[u].stage(kind, k, g)
        else:
            pieces[name](*numbers)
    trade(4, rf, rf).wait_recv()

    def out_block(i, _):
        r = pl.ds(pl.multiple_of(i * 16, 16), 16)
        a = (pf[core, r, :].astype(F32) + rf[core, r, :].astype(F32)).astype(BF16).astype(F32)
        b = (pf[1 - core, r, :].astype(F32) + rf[1 - core, r, :].astype(F32)).astype(BF16).astype(F32)
        inv = norm_rows(a, b, 2 * HALF)
        out[0, r, :] = (mid[core, r, :].astype(F32) + a * inv * gains[core, 3]).astype(BF16)
        return 0

    lax.fori_loop(0, ROWS // 16, out_block, 0, unroll=4)
    swap_x.wait_send()
    swap_g.wait_send()
    swap_s.wait_send()
    trade(3, pm, pm).wait_send()
    trade(4, pf, pf).wait_send()
    for u in units:
        u.drain()


def per_device(*args):
    arrays = [a.reshape(1, -1) if a.ndim == 1 else a for a in args]
    sems = pltpu.SemaphoreType.DMA
    return pl.pallas_call(
        kernel,
        out_shape=pltpu.VMEM((1, ROWS, HALF), BF16),
        in_specs=[pl.BlockSpec(memory_space=pl.ANY)] * len(arrays),
        out_specs=pl.BlockSpec(memory_space=pltpu.VMEM),
        scratch_shapes=[
            pltpu.VMEM((3, 2, 4, 4, 64, HALF), BF16),
            pltpu.VMEM((3, 2, 4, 4, 64, HID), BF16),
            pltpu.VMEM((2, ROWS, HALF), BF16),
            pltpu.VMEM((2, ROWS, HALF), BF16),
            pltpu.VMEM((ROWS, HALF), F32),
            pltpu.VMEM((32 + ROWS, HALF), F32),
            pltpu.VMEM((ROWS, HALF), BF16),
            pltpu.VMEM((2, ROWS, HALF), BF16),
            pltpu.VMEM((2, ROWS, HALF), BF16),
            pltpu.VMEM((2, ROWS, HALF), BF16),
            pltpu.VMEM((2, ROWS, HALF), BF16),
            pltpu.VMEM((2, ROWS, HALF), BF16),
            pltpu.VMEM((8 + ROWS, HID), F32),
            pltpu.VMEM((8 + ROWS, HID), F32),
            pltpu.VMEM((ROWS, HID), BF16),
            pltpu.VMEM((2, 2, ROWS, 128), F32),
            pltpu.VMEM((2, 6, 1, HALF), F32),
            pltpu.VMEM((31, HALF), BF16),
            pltpu.VMEM((32, HALF), F32),
            pltpu.VMEM((3, HID), BF16),
            pltpu.VMEM((3, HID), BF16),
            sems((len(UNITS),)),
            sems((sum(Unit.semaphores(cols, split) for _, _, _, cols, split in UNITS),)),
            sems((7,)),
            sems((5,)),
            sems((5,)),
        ],
        compiler_params=pltpu.CompilerParams(collective_id=0, has_side_effects=True, vmem_limit_bytes=60 << 20),
    )(*arrays)


def solution(mesh):
    rows = P(("rep", "fs"), None, "tp")
    vector, matrix, taps = P("tp"), P("fs", "tp"), P(None, "tp")
    placed = (
        rows, vector, matrix, matrix, taps, vector, vector, matrix, vector, vector,
        matrix, matrix, taps, taps, matrix, vector,
    )
    return jax.shard_map(per_device, mesh=mesh, in_specs=placed, out_specs=rows, check_vma=False)
```

time: 145 us -> 127 us (0.88)
  Pallas kernels: 142 us -> 126 us
    pallas_call x1, Pallas kernels: 142 us -> 126 us  [per_device(): pl.pallas_call(kernel, out_shape=pltpu.VMEM((1, ROWS, HALF), BF16), in_sp...]
where the time goes in v2:
time: 127 us
  Pallas kernels  126 us (99%)
    pallas_call x1, Pallas kernels, per_device(): pl.pallas_call(kernel, out_shape=pltpu.VMEM((1, ROWS, HALF), BF16), in_sp...  126 us

profile of v2, /device:TPU:1, one launch (start us, length us, event | category | flops | bytes accessed | tf_op | source)
XLA Modules:
  0.0 127.1 jit_solution(13705011900461048215)
XLA Ops:
  0.0 126.1 %shard_map.154 = bf16[1,512,1024]{2,1,0:T(8,128)(2,1)S(1)} custom-call(bf16[1,512,1024]{2,1,0:T(8,128)(2,1)} %stream_in.1, f32[1,1024]{1,0:T(1,128)} %bitcast.6, bf16[64,1024]{1,0:T(8,128)(2,1)} %value_in.1, bf16[64,1024]{1,0:T(8,128)(2,1)} %gate_in.1, bf16[31,1024]{1,0:T(8,128)(2,1)} %taps_in.1, f32[1,1024]{1,0:T(1,128)} %bitcast.7, f32[1,1024]{1,0:T(1,128)} %bitcast.8, ...), custom_call_target="tpu_custom_call" | custom-call | tf_op jit(solution)/shard_map/pallas_call | solution.py:397
  126.2 1.0 copy.18

commit v3 on v2

v3 whole, which is shorter than its diff:
```python
import functools

import jax
import jax.numpy as jnp
from jax import lax
from jax.experimental import pallas as pl
from jax.experimental.pallas import tpu as pltpu
from jax.sharding import PartitionSpec as P

EPS = 1e-06
MESH = pl.DeviceIdType.MESH
F32, BF16 = jnp.float32, jnp.bfloat16

class Place:
    def __init__(s):
        fs = lax.axis_index("fs"); zh = lax.axis_index("rep")
        s.core = lax.axis_index("tp")
        s.x = fs % 4; s.y = (fs // 4) % 4; s.zl = fs // 16
        s.z = zh * 2 + s.zl
    def dev(s, dx=0, dy=0, dz=0):
        x = (s.x + dx + 4) % 4; y = (s.y + dy + 4) % 4; z = (s.z + dz + 4) % 4
        return (z // 2, (z % 2) * 16 + y * 4 + x, s.core)
    def pair(s, core):
        return (lax.axis_index("rep"), (1 - s.zl) * 16 + s.y * 4 + s.x, core)

    def partner(s):
        return (lax.axis_index("rep"), lax.axis_index("fs"), 1 - s.core)

class Unit:
    WAITS = (6, 7)

    def __init__(s, place, buf, m, lo, cols, split, ssem, rsem, u, base, turns, away):
        s.turns, s.away = turns, away
        s.p, s.buf, s.m = place, buf, m
        s.c1, s.c2, s.all_columns = pl.ds(lo, split), pl.ds(lo + split, cols - split), pl.ds(lo, cols)
        s.ssem, s.rsem = ssem.at[u], rsem
        s.base = (base, base + (13 if split else 0))

    @staticmethod
    def semaphores(cols, split):
        return (13 if split else 0) + (14 if split < cols else 0)

    def region(s, g, kind, part, content, da, db):
        rows = pl.ds(32 * g + 16 * max(part, 0), 32 if part < 0 else 16)
        cols = s.c1 if kind == 1 else s.c2
        z = slice(None) if content is None else content
        first, second = (s.p.x, s.p.y) if g == 0 else (s.p.y, s.p.x)
        a = slice(None) if da is None else (first + da + 4) % 4
        b = (second + db + 4) % 4
        y, x = (b, a) if g == 0 else (a, b)
        return s.buf.at[s.m, z, y, x, rows, cols]

    def copy(s, n, region, dev):
        return pltpu.make_async_remote_copy(
            src_ref=region, dst_ref=region, send_sem=s.ssem, recv_sem=s.rsem.at[n], device_id=dev, device_id_type=MESH
        )

    def drain(s):
        whole = s.buf.reshape(3, 32, *s.buf.shape[4:]).at[s.m, pl.ds(0, 31), :, s.all_columns]
        s.copy(0, whole, s.p.dev()).wait_send()

    def stage(s, kind, k, g):
        if (s.c1 if kind == 1 else s.c2).size == 0:
            return
        mine, other, R = s.p.zl, 1 - s.p.zl, functools.partial(s.region, g, kind)
        sem = s.base[kind - 1] + g * s.WAITS[kind - 1]
        up = s.turns[g] * (1 - 2 * s.p.zl)
        signs = ((0, 1), (1, -1))

        def send(n, region, da=0, db=0, dz=0):
            s.copy(sem + n, region, s.p.dev(da, db, dz) if g == 0 else s.p.dev(db, da, dz)).start()

        def to_z(region):
            s.copy(s.base[0] + 12, region, s.p.dev(0, 0, up)).start()

        def wait(n, region):
            s.copy(sem + n, region, s.p.dev()).wait_recv()

        if (kind, k) == (1, 0):
            for i, d in signs:
                send(i, R(-1, mine, 0, 0), d)
        elif (kind, k) == (1, 1):
            for i, d in signs:
                wait(i, R(-1, mine, -d, 0))
                send(2, R(i, mine, -d, 0), d)
        elif (kind, k) == (1, 2):
            wait(2, R(-1, mine, 2, 0))
            for i, d in signs:
                send(3 + i, R(-1, mine, None, 0), 0, d)
            to_z(R(-1, mine, None, 0))
        elif (kind, k) == (1, 3):
            for i, d in signs:
                wait(3 + i, R(-1, mine, None, -d))
                send(5, R(i, mine, None, -d), 0, d)
                to_z(R(-1, mine, None, -d))
        elif (kind, k) == (1, 4):
            wait(5, R(-1, mine, None, 2))
            to_z(R(-1, mine, None, 2))
        elif (kind, k) == (1, 5):
            if g == 0:
                wait(12, s.buf.at[s.m, other, :, :, :, s.c1])
        elif (kind, k) == (2, 0):
            own = R(-1, mine, 0, 0)
            source = own if s.away is None else s.away.at[s.m, pl.ds(32 * g, 32)]
            pltpu.make_async_remote_copy(
                src_ref=source, dst_ref=own, send_sem=s.ssem, recv_sem=s.rsem.at[sem], device_id=s.p.dev(0, 0, up), device_id_type=MESH
            ).start()
        elif (kind, k) == (2, 1):
            wait(0, R(-1, other, 0, 0))
            for i, d in signs:
                send(1 + i, R(-1, None, 0, 0), d)
        elif (kind, k) == (2, 2):
            for i, d in signs:
                wait(1 + i, R(-1, None, -d, 0))
                send(3, R(i, None, -d, 0), d)
        elif (kind, k) == (2, 3):
            wait(3, R(-1, None, 2, 0))
            for i, d in signs:
                send(4 + i, R(-1, None, None, 0), 0, d)
        elif (kind, k) == (2, 4):
            for i, d in signs:
                wait(4 + i, R(-1, None, None, -d))
                send(6, R(i, None, None, -d), 0, d)
        elif (kind, k) == (2, 5):
            wait(6, R(-1, None, None, 2))


def barrier(p):
    sem = pltpu.get_barrier_semaphore()
    ds = [p.dev(1), p.dev(-1), p.dev(0, 1), p.dev(0, -1), p.dev(0, 0, 1), p.dev(0, 0, -1), p.partner(), p.pair(1 - p.core)]
    for d in ds:
        pl.semaphore_signal(sem, inc=1, device_id=d, device_id_type=MESH)
    pl.semaphore_wait(sem, len(ds))


QUARTER = 512
UNITS = (
    (0, pl.ds(0, 2), 0, QUARTER, 0, (1, -1)),
    (0, 2, 0, QUARTER, 0, (1, -1)),
    (1, pl.ds(0, 2), 0, 768, 384, (-1, 1)),
    (1, pl.ds(0, 2), 768, 640, 384, (-1, -1)),
    (1, 2, 0, 640, 640, (-1, 1)),
    (1, 2, 640, 768, 128, (1, 1)),
)
DOWN = (0, 640, 1408)
SCHEDULE = (
    ("u", 0, 2, 0), ("start",), ("u", 2, 1, 0), ("u", 3, 1, 0), ("u", 4, 1, 0), ("u", 5, 1, 0), ("u", 0, 2, 1),
    ("u", 1, 2, 0), ("u", 2, 1, 1), ("norm",), ("u", 1, 2, 1), ("u", 2, 2, 0), ("u", 3, 1, 1), ("u", 0, 2, 2),
    ("u", 2, 1, 2), ("u", 0, 2, 3), ("u", 1, 2, 2), ("u", 0, 2, 4), ("u", 1, 2, 3), ("u", 2, 1, 3), ("fwd",),
    ("u", 2, 2, 1), ("u", 3, 1, 2), ("u", 3, 2, 0), ("u", 4, 1, 1), ("u", 0, 2, 5), ("glu", 0), ("glu", 1), ("glu", 2),
    ("glu", 3), ("conv", 0), ("u", 1, 2, 4), ("conv", 1), ("u", 2, 1, 4), ("conv", 2), ("u", 2, 2, 2), ("conv", 3),
    ("stats",), ("u", 3, 2, 1), ("u", 5, 1, 1), ("u", 5, 2, 0), ("u", 4, 1, 2), ("u", 1, 2, 5), ("act",),
    ("u", 2, 1, 5), ("u", 2, 2, 3), ("u", 3, 1, 3), ("proj", 0), ("u", 3, 2, 2), ("u", 5, 1, 2), ("u", 5, 2, 1),
    ("proj", 1), ("red",), ("proj", 2), ("u", 2, 2, 4), ("rz", 0), ("mid", 0), ("u", 3, 1, 4), ("u", 3, 2, 3),
    ("u", 4, 1, 3), ("u", 5, 1, 3), ("u", 5, 2, 2), ("rz", 1), ("mid", 1), ("u", 2, 2, 5), ("rz", 2), ("mid", 2),
    ("u", 3, 1, 5), ("u", 3, 2, 4), ("u", 4, 1, 4), ("rz", 3), ("u", 5, 1, 4), ("u", 5, 2, 3), ("mid", 3), ("up", 0),
    ("up", 1), ("u", 3, 2, 5), ("up", 2), ("hid", 0), ("hid", 1), ("up", 3), ("up", 4), ("u", 5, 2, 4), ("up", 5),
    ("hid", 2), ("hid", 3), ("u", 4, 1, 5), ("down", 0), ("u", 5, 1, 5), ("u", 5, 2, 5), ("down", 1),
)
ROWS = 512
HALF = 1024
HID = 1408


def norm_rows(a, b, width):
    total = jnp.sum(a * a, axis=1, keepdims=True) + jnp.sum(b * b, axis=1, keepdims=True)
    return lax.rsqrt(total * (1.0 / width) + EPS)


def kernel(
    stream_in, pre_mix_in, value_in, gate_in, taps_in, bias_in, chan_in, proj_in, post_mix_in, pre_ffn_in,
    up_gate_in, up_value_in, gate_taps_in, value_taps_in, down_in, post_ffn_in,
    out,
    wm, wf, away, xs, xn, xq, val, glu, act, pm, rm, pq, rq, rz, pf, rf, mid, upg, upv, hid, st, mi, gains, taps_b, taps, gtaps_b, vtaps_b, acc,
    ssem, rsem, lsem, psend, precv,
):
    p = Place()
    core = p.core
    partner = p.partner()

    def trade(n, src, dst, device=None):
        return pltpu.make_async_remote_copy(
            src_ref=src, dst_ref=dst, send_sem=psend.at[n], recv_sem=precv.at[n], device_id=device or partner, device_id_type=MESH
        )

    mine = pl.ds(pl.multiple_of(QUARTER * p.zl, QUARTER), QUARTER)
    theirs = pl.ds(pl.multiple_of(QUARTER * (1 - p.zl), QUARTER), QUARTER)
    twin = p.pair(core)

    def load(src, dst, n):
        return pltpu.make_async_copy(src, dst, lsem.at[n])

    for i, w in enumerate((value_in, gate_in, proj_in)):
        load(w.at[:, mine], wm.at[i, p.zl, p.y, p.x], 0).start()
        load(w.at[:, theirs], away.at[i], 7).start()
    for i, w in enumerate((up_gate_in, up_value_in, down_in)):
        load(w, wf.at[i, p.zl, p.y, p.x], 1).start()
    for i, v in enumerate((pre_mix_in, post_mix_in, pre_ffn_in, post_ffn_in, bias_in, chan_in)):
        load(v, gains.at[core, i], 2).start()
    small = [load(stream_in.at[0], xs.at[core], 3), load(taps_in.at[:, mine], taps_b, 4), load(gate_taps_in, gtaps_b, 5), load(value_taps_in, vtaps_b, 6)]
    for c in small:
        c.start()
    barrier(p)
    for n, whole in ((0, wm.at[:, p.zl, p.y, p.x]), (1, wf.at[:, p.zl, p.y, p.x]), (7, away)):
        load(whole, whole, n).wait()
    units, base = [], 0
    for u, (ffn, m, lo, cols, split, turns) in enumerate(UNITS):
        units.append(Unit(p, wf if ffn else wm, m, lo, cols, split, ssem, rsem, u, base, turns, None if ffn else away))
        base += Unit.semaphores(cols, split)
    swap_x = trade(0, xs.at[core], xs.at[core])
    swap_g = trade(1, gains.at[core], gains.at[core])

    def start():
        load(gains.at[core], gains.at[core], 2).wait()
        for c in small:
            c.wait()
        swap_x.start()
        swap_g.start()
        taps[0:31, :] = taps_b[...].astype(F32)
        glu[:, 0:32, :] = jnp.zeros((2, 32, QUARTER), F32)
        upg[0:8, :] = jnp.zeros((8, HID), F32)
        upv[0:8, :] = jnp.zeros((8, HID), F32)

    def first_norm(i, _):
        r = pl.ds(pl.multiple_of(i * 16, 16), 16)
        a, b = xs[0, r, :].astype(F32), xs[1, r, :].astype(F32)
        inv = norm_rows(a, b, 2 * HALF)
        xn[0, r, :] = (a * inv * gains[0, 0]).astype(BF16)
        xn[1, r, :] = (b * inv * gains[1, 0]).astype(BF16)
        return 0

    def norm():
        trade(0, xs.at[1 - core], xs.at[1 - core]).wait_recv()
        trade(1, gains.at[1 - core], gains.at[1 - core]).wait_recv()
        lax.fori_loop(0, ROWS // 16, first_norm, 0, unroll=2)
        trade(5, xn.at[core], xq.at[core], twin).start()

    def forward():
        trade(5, xq.at[core], xq.at[core], twin).wait_recv()
        trade(6, xq.at[core], xq.at[core]).start()

    def product(lhs, buf, m, c):
        w0 = buf[m, 0, :, :, :, c].reshape(HALF, c.size)
        w1 = buf[m, 1, :, :, :, c].reshape(HALF, c.size)
        return jnp.dot(lhs[0], w0, preferred_element_type=F32) + jnp.dot(lhs[1], w1, preferred_element_type=F32)

    def glu_piece(i):
        if i == 2:
            trade(6, xq.at[1 - core], xq.at[1 - core]).wait_recv()
        c = pl.ds(256 * (i % 2), 256)
        lhs = xq if i // 2 else xn
        v, g = product(lhs, wm, 0, c), product(lhs, wm, 1, c)
        glu[i // 2, 32 : 32 + ROWS, c] = (v * jax.nn.sigmoid(g)).astype(BF16).astype(F32)

    def conv(piece):
        def conv_block(i, _):
            first = 256 * (piece % 2) + 128 * (i // 8)
            c = pl.ds(pl.multiple_of(first, 128), 128)
            t = pl.multiple_of((i % 8) * 64, 64)
            g = glu[piece // 2, pl.ds(t, 96), c]
            bias = gains[core, 4, :, pl.ds(pl.multiple_of(QUARTER * p.zl + first, 128), 128)]
            total = jnp.broadcast_to(bias, (64, 128))
            for k in range(8):
                part = None
                rows = 72 if k else 64
                for j in range(31):
                    if (2 + j) % 8 == k:
                        at = (2 + j) // 8 * 8
                        term = taps[j : j + 1, c] * g[at : at + rows]
                        part = term if part is None else part + term
                total = total + part[k : k + 64]
            val[piece // 2, pl.ds(t, 64), c] = total
            return 0

        lax.fori_loop(0, 16, conv_block, 0)

    lane = lax.broadcasted_iota(jnp.int32, (32, 128), 1)
    owner = (p.zl, 1 - p.zl)
    slot = 2 * p.zl + core
    stats_to = ((2, partner, 2 * p.zl + 1 - core), (7, twin, 2 * (1 - p.zl) + core), (8, p.pair(1 - core), 2 * (1 - p.zl) + 1 - core))

    def stats():
        def block(i, tiles):
            r = pl.ds(pl.multiple_of(i * 32, 32), 32)
            means, squares = tiles
            for q in range(2):
                v = val[q, r, :]
                mean = jnp.sum(v, axis=1, keepdims=True) * (1.0 / QUARTER)
                d = v - mean
                here = lane == 16 * owner[q] + i
                means = jnp.where(here, mean, means)
                squares = jnp.where(here, jnp.sum(d * d, axis=1, keepdims=True), squares)
            return means, squares

        zero = jnp.zeros((32, 128), F32)
        st[slot, 0], st[slot, 1] = lax.fori_loop(0, ROWS // 32, block, (zero, zero), unroll=2)
        for n, device, _ in stats_to:
            trade(n, st.at[slot], st.at[slot], device).start()

    def activate():
        for n, device, source in stats_to:
            trade(n, st.at[source], st.at[source], device).wait_recv()
        mean = (st[0, 0] + st[1, 0] + st[2, 0] + st[3, 0]) * 0.25
        square = jnp.zeros((32, 128), F32)
        for k in range(4):
            d = st[k, 0] - mean
            square = square + (st[k, 1] + d * d * QUARTER)
        mi[0] = mean
        mi[1] = lax.rsqrt(square * (0.5 / HALF) + EPS)
        gain = gains[core, 5, :, mine]

        def block(i, _):
            r = pl.ds(pl.multiple_of(i * 32, 32), 32)
            for q in range(2):
                here = lane == 16 * owner[q] + i
                m = jnp.sum(jnp.where(here, mi[0], 0.0), axis=1, keepdims=True)
                inv = jnp.sum(jnp.where(here, mi[1], 0.0), axis=1, keepdims=True)
                act[q, r, :] = jax.nn.silu((val[q, r, :] - m) * inv * gain).astype(BF16)
            return 0

        lax.fori_loop(0, ROWS // 32, block, 0, unroll=2)

    def region(ref, i):
        return ref.at[i // 2, :, pl.ds(512 * (i % 2), 512)]

    def rows_product(lhs, buf, part, total, mine, theirs, base, lo, hi):
        def send(i):
            trade(base, region(mine, i), region(theirs, i)).start()

        for i in range(lo, hi):
            h, n = i // 2, i % 2
            w = buf[2, h, 2 * n : 2 * n + 2, :, :, part].reshape(512, part.size)
            c = pl.ds(512 * n, 512)
            term = lax.dot_general(lhs[:, part], w, (((1,), (1,)), ((), ())), preferred_element_type=F32)
            if mine is None:
                total[h, :, c] = term
                continue
            mine[h, :, c] = (term if total is None else total[h, :, c] + term).astype(BF16)
            if i > lo and theirs is not None:
                send(i - 1)
        if mine is not None and theirs is not None:
            send(hi - 1)

    def middle_block(i, _):
        r = pl.ds(pl.multiple_of(i * 16, 16), 16)
        a = (pm[0, r, :].astype(F32) + rm[0, r, :].astype(F32) + rz[0, r, :].astype(F32)).astype(BF16).astype(F32)
        b = (pm[1, r, :].astype(F32) + rm[1, r, :].astype(F32) + rz[1, r, :].astype(F32)).astype(BF16).astype(F32)
        inv = norm_rows(a, b, 2 * HALF)
        a = (xs[0, r, :].astype(F32) + a * inv * gains[0, 1]).astype(BF16)
        b = (xs[1, r, :].astype(F32) + b * inv * gains[1, 1]).astype(BF16)
        mid[0, r, :] = a
        mid[1, r, :] = b
        a, b = a.astype(F32), b.astype(F32)
        inv = norm_rows(a, b, 2 * HALF)
        xn[0, r, :] = (a * inv * gains[0, 2]).astype(BF16)
        xn[1, r, :] = (b * inv * gains[1, 2]).astype(BF16)
        return 0

    def up_block(c):
        g, v = product(xn, wf, 0, c), product(xn, wf, 1, c)
        upg[8 : 8 + ROWS, c] = g.astype(BF16).astype(F32)
        upv[8 : 8 + ROWS, c] = v.astype(BF16).astype(F32)

    def hidden_block(i, _):
        c = pl.ds(pl.multiple_of((i // 8) * 128, 128), 128)
        t = pl.multiple_of((i % 8) * 64, 64)
        g, v = upg[pl.ds(t, 72), c], upv[pl.ds(t, 72), c]
        kg, kv = gtaps_b[:, c].astype(F32), vtaps_b[:, c].astype(F32)
        gc = kg[0:1] * g[6:70] + kg[1:2] * g[7:71] + kg[2:3] * g[8:72]
        vc = kv[0:1] * v[6:70] + kv[1:2] * v[7:71] + kv[2:3] * v[8:72]
        hid[pl.ds(t, 64), c] = (jax.nn.silu(gc) * vc).astype(BF16)
        return 0

    def project(i):
        part = pl.ds(0, QUARTER)
        if i:
            rows_product(act.at[0], wm, part, None, pm, rm, 3, 2 * i - 2, 2 * i)
            return
        rows_product(act.at[1], wm, part, None, pq, None, None, 0, 4)
        trade(17, pq.at[1 - core], rq).start()

    def chunk(k):
        return pl.ds(128 * k, 128)

    def reduce():
        trade(17, rq, rq).wait_recv()
        for k in range(4):

            def block(i, _):
                r = pl.ds(pl.multiple_of(i * 32, 32), 32)
                pq[core, r, :] = (pq[core, r, :].astype(F32) + rq[r, :].astype(F32)).astype(BF16)
                return 0

            lax.fori_loop(4 * k, 4 * k + 4, block, 0, unroll=2)
            trade(9 + k, pq.at[core, chunk(k)], rz.at[core, chunk(k)], twin).start()

    def relay(k):
        here = rz.at[core, chunk(k)]
        trade(9 + k, here, here, twin).wait_recv()
        trade(13 + k, here, here).start()

    def middle(k):
        if k == 0:
            trade(3, rm, rm).wait_recv()
            trade(5, xn.at[core], xq.at[core], twin).wait_send()
        there = rz.at[1 - core, chunk(k)]
        trade(13 + k, there, there).wait_recv()
        lax.fori_loop(8 * k, 8 * k + 8, middle_block, 0, unroll=2)

    def up(i):
        up_block(pl.ds(256 * i, min(256, HID - 256 * i)))

    def hidden(i):
        lo, hi = ((0, 24), (24, 48), (48, 68), (68, 88))[i]
        lax.fori_loop(lo, hi, hidden_block, 0)

    def down(i):
        part = pl.ds(DOWN[i], DOWN[i + 1] - DOWN[i])
        last = i + 2 == len(DOWN)
        rows_product(hid, wf, part, acc if i < 1 < len(DOWN) - 1 or i else None, pf if last else None, rf, 4, 0, 4)

    pieces = dict(
        start=start, norm=norm, glu=glu_piece, conv=conv, stats=stats, act=activate, proj=project, red=reduce, rz=relay, fwd=forward, mid=middle, up=up, hid=hidden, down=down
    )
    for name, *numbers in SCHEDULE:
        if name == "u":
            u, kind, k = numbers
            for g in range(2):
                units[u].stage(kind, k, g)
        else:
            pieces[name](*numbers)
    trade(4, rf, rf).wait_recv()

    def out_block(i, _):
        r = pl.ds(pl.multiple_of(i * 16, 16), 16)
        a = (pf[core, r, :].astype(F32) + rf[core, r, :].astype(F32)).astype(BF16).astype(F32)
        b = (pf[1 - core, r, :].astype(F32) + rf[1 - core, r, :].astype(F32)).astype(BF16).astype(F32)
        inv = norm_rows(a, b, 2 * HALF)
        out[0, r, :] = (mid[core, r, :].astype(F32) + a * inv * gains[core, 3]).astype(BF16)
        return 0

    lax.fori_loop(0, ROWS // 16, out_block, 0, unroll=4)
    swap_x.wait_send()
    swap_g.wait_send()
    for n, device, _ in stats_to:
        trade(n, st.at[slot], st.at[slot], device).wait_send()
    trade(6, xq.at[core], xq.at[core]).wait_send()
    trade(17, pq.at[1 - core], rq).wait_send()
    for k in range(4):
        trade(9 + k, pq.at[core, chunk(k)], rz.at[core, chunk(k)], twin).wait_send()
        trade(13 + k, rz.at[core, chunk(k)], rz.at[core, chunk(k)]).wait_send()
    trade(3, pm, pm).wait_send()
    trade(4, pf, pf).wait_send()
    for u in units:
        u.drain()


def per_device(*args):
    arrays = [a.reshape(1, -1) if a.ndim == 1 else a for a in args]
    sems = pltpu.SemaphoreType.DMA
    return pl.pallas_call(
        kernel,
        out_shape=pltpu.VMEM((1, ROWS, HALF), BF16),
        in_specs=[pl.BlockSpec(memory_space=pl.ANY)] * len(arrays),
        out_specs=pl.BlockSpec(memory_space=pltpu.VMEM),
        scratch_shapes=[
            pltpu.VMEM((3, 2, 4, 4, 64, QUARTER), BF16),
            pltpu.VMEM((3, 2, 4, 4, 64, HID), BF16),
            pltpu.VMEM((3, 64, QUARTER), BF16),
            pltpu.VMEM((2, ROWS, HALF), BF16),
            pltpu.VMEM((2, ROWS, HALF), BF16),
            pltpu.VMEM((2, ROWS, HALF), BF16),
            pltpu.VMEM((2, ROWS, QUARTER), F32),
            pltpu.VMEM((2, 32 + ROWS, QUARTER), F32),
            pltpu.VMEM((2, ROWS, QUARTER), BF16),
            pltpu.VMEM((2, ROWS, HALF), BF16),
            pltpu.VMEM((2, ROWS, HALF), BF16),
            pltpu.VMEM((2, ROWS, HALF), BF16),
            pltpu.VMEM((ROWS, HALF), BF16),
            pltpu.VMEM((2, ROWS, HALF), BF16),
            pltpu.VMEM((2, ROWS, HALF), BF16),
            pltpu.VMEM((2, ROWS, HALF), BF16),
            pltpu.VMEM((2, ROWS, HALF), BF16),
            pltpu.VMEM((8 + ROWS, HID), F32),
            pltpu.VMEM((8 + ROWS, HID), F32),
            pltpu.VMEM((ROWS, HID), BF16),
            pltpu.VMEM((4, 2, 32, 128), F32),
            pltpu.VMEM((2, 32, 128), F32),
            pltpu.VMEM((2, 6, 1, HALF), F32),
            pltpu.VMEM((31, QUARTER), BF16),
            pltpu.VMEM((32, QUARTER), F32),
            pltpu.VMEM((3, HID), BF16),
            pltpu.VMEM((3, HID), BF16),
            pltpu.VMEM((2, ROWS, HALF), F32),
            sems((len(UNITS),)),
            sems((sum(Unit.semaphores(cols, split) for _, _, _, cols, split, _ in UNITS),)),
            sems((8,)),
            sems((18,)),
            sems((18,)),
        ],
        compiler_params=pltpu.CompilerParams(collective_id=0, has_side_effects=True, vmem_limit_bytes=62 << 20),
    )(*arrays)


def solution(mesh):
    rows = P(("rep", "fs"), None, "tp")
    vector, matrix, taps = P("tp"), P("fs", "tp"), P(None, "tp")
    placed = (
        rows, vector, matrix, matrix, taps, vector, vector, matrix, vector, vector,
        matrix, matrix, taps, taps, matrix, vector,
    )
    return jax.shard_map(per_device, mesh=mesh, in_specs=placed, out_specs=rows, check_vma=False)
```

time: 127 us -> 118 us (0.929)
  Pallas kernels: 126 us -> 117 us
    pallas_call x1, Pallas kernels: 126 us -> 117 us  [per_device(): pl.pallas_call(kernel, out_shape=pltpu.VMEM((1, ROWS, HALF), BF16), in_sp...]
where the time goes in v3:
time: 118 us
  Pallas kernels  117 us (99%)
    pallas_call x1, Pallas kernels, per_device(): pl.pallas_call(kernel, out_shape=pltpu.VMEM((1, ROWS, HALF), BF16), in_sp...  117 us

profile of v3, /device:TPU:1, one launch (start us, length us, event | category | flops | bytes accessed | tf_op | source)
XLA Modules:
  0.0 117.5 jit_solution(13856879477599944750)
XLA Ops:
  0.0 116.5 %shard_map.154 = bf16[1,512,1024]{2,1,0:T(8,128)(2,1)S(1)} custom-call(bf16[1,512,1024]{2,1,0:T(8,128)(2,1)} %stream_in.1, f32[1,1024]{1,0:T(1,128)} %bitcast.6, bf16[64,1024]{1,0:T(8,128)(2,1)} %value_in.1, bf16[64,1024]{1,0:T(8,128)(2,1)} %gate_in.1, bf16[31,1024]{1,0:T(8,128)(2,1)} %taps_in.1, f32[1,1024]{1,0:T(1,128)} %bitcast.7, f32[1,1024]{1,0:T(1,128)} %bitcast.8, ...), custom_call_target="tpu_custom_call" | custom-call | tf_op jit(solution)/shard_map/pallas_call | solution.py:461
  116.6 1.0 copy.18

commit v4 on v3

--- a/solution.py
+++ b/solution.py
@@ -144,18 +144,18 @@
 )
 DOWN = (0, 640, 1408)
 SCHEDULE = (
-    ("u", 0, 2, 0), ("start",), ("u", 2, 1, 0), ("u", 3, 1, 0), ("u", 4, 1, 0), ("u", 5, 1, 0), ("u", 0, 2, 1),
-    ("u", 1, 2, 0), ("u", 2, 1, 1), ("norm",), ("u", 1, 2, 1), ("u", 2, 2, 0), ("u", 3, 1, 1), ("u", 0, 2, 2),
-    ("u", 2, 1, 2), ("u", 0, 2, 3), ("u", 1, 2, 2), ("u", 0, 2, 4), ("u", 1, 2, 3), ("u", 2, 1, 3), ("fwd",),
-    ("u", 2, 2, 1), ("u", 3, 1, 2), ("u", 3, 2, 0), ("u", 4, 1, 1), ("u", 0, 2, 5), ("glu", 0), ("glu", 1), ("glu", 2),
-    ("glu", 3), ("conv", 0), ("u", 1, 2, 4), ("conv", 1), ("u", 2, 1, 4), ("conv", 2), ("u", 2, 2, 2), ("conv", 3),
-    ("stats",), ("u", 3, 2, 1), ("u", 5, 1, 1), ("u", 5, 2, 0), ("u", 4, 1, 2), ("u", 1, 2, 5), ("act",),
-    ("u", 2, 1, 5), ("u", 2, 2, 3), ("u", 3, 1, 3), ("proj", 0), ("u", 3, 2, 2), ("u", 5, 1, 2), ("u", 5, 2, 1),
-    ("proj", 1), ("red",), ("proj", 2), ("u", 2, 2, 4), ("rz", 0), ("mid", 0), ("u", 3, 1, 4), ("u", 3, 2, 3),
-    ("u", 4, 1, 3), ("u", 5, 1, 3), ("u", 5, 2, 2), ("rz", 1), ("mid", 1), ("u", 2, 2, 5), ("rz", 2), ("mid", 2),
-    ("u", 3, 1, 5), ("u", 3, 2, 4), ("u", 4, 1, 4), ("rz", 3), ("u", 5, 1, 4), ("u", 5, 2, 3), ("mid", 3), ("up", 0),
-    ("up", 1), ("u", 3, 2, 5), ("up", 2), ("hid", 0), ("hid", 1), ("up", 3), ("up", 4), ("u", 5, 2, 4), ("up", 5),
-    ("hid", 2), ("hid", 3), ("u", 4, 1, 5), ("down", 0), ("u", 5, 1, 5), ("u", 5, 2, 5), ("down", 1),
+    ("u", 0, 2, 0), ("start",), ("u", 4, 1, 0), ("u", 3, 1, 0), ("u", 5, 1, 0), ("u", 1, 2, 0), ("u", 2, 1, 0),
+    ("u", 3, 2, 0), ("u", 0, 2, 1), ("u", 2, 1, 1), ("u", 1, 2, 1), ("u", 2, 2, 0), ("u", 5, 2, 0), ("u", 3, 1, 1),
+    ("norm",), ("u", 0, 2, 2), ("u", 2, 1, 2), ("u", 1, 2, 2), ("u", 0, 2, 3), ("u", 2, 1, 3), ("u", 0, 2, 4), ("fwd",),
+    ("u", 5, 1, 1), ("u", 1, 2, 3), ("u", 3, 2, 1), ("u", 3, 1, 2), ("u", 2, 2, 1), ("u", 2, 1, 4), ("u", 4, 1, 1),
+    ("u", 0, 2, 5), ("glu", 0), ("glu", 1), ("glu", 2), ("conv", 1), ("conv", 0), ("u", 1, 2, 4), ("conv", 2),
+    ("u", 5, 1, 2), ("glu", 3), ("conv", 3), ("stats",), ("u", 3, 1, 3), ("u", 2, 2, 2), ("u", 1, 2, 5), ("u", 4, 1, 2),
+    ("act",), ("proj", 0), ("u", 2, 2, 3), ("u", 5, 2, 1), ("u", 3, 2, 2), ("proj", 1), ("u", 3, 1, 4), ("red",),
+    ("u", 2, 2, 4), ("rz", 0), ("proj", 2), ("mid", 0), ("u", 3, 2, 3), ("u", 2, 2, 5), ("rz", 1), ("u", 4, 1, 3),
+    ("rz", 2), ("u", 5, 2, 2), ("u", 3, 2, 4), ("u", 2, 1, 5), ("mid", 1), ("mid", 2), ("u", 4, 1, 4), ("rz", 3),
+    ("u", 5, 2, 3), ("u", 3, 1, 5), ("u", 5, 1, 3), ("mid", 3), ("up", 0), ("u", 3, 2, 5), ("up", 1), ("up", 2),
+    ("up", 3), ("up", 4), ("hid", 1), ("u", 5, 2, 4), ("up", 5), ("u", 5, 1, 4), ("u", 4, 1, 5), ("hid", 2), ("hid", 3),
+    ("hid", 0), ("down", 0), ("u", 5, 1, 5), ("u", 5, 2, 5), ("down", 1),
 )
 ROWS = 512
 HALF = 1024
@@ -412,7 +412,7 @@
 
     def hidden(i):
         lo, hi = ((0, 24), (24, 48), (48, 68), (68, 88))[i]
-        lax.fori_loop(lo, hi, hidden_block, 0)
+        lax.fori_loop(lo, hi, hidden_block, 0, unroll=2)
 
     def down(i):
         part = pl.ds(DOWN[i], DOWN[i + 1] - DOWN[i])

time: 118 us -> 117 us (level)
  no operation moved by 1% of the time
where the time goes in v4:
time: 117 us
  Pallas kernels  116 us (99%)
    pallas_call x1, Pallas kernels, per_device(): pl.pallas_call(kernel, out_shape=pltpu.VMEM((1, ROWS, HALF), BF16), in_sp...  116 us

profile of v4, /device:TPU:1, one launch (start us, length us, event | category | flops | bytes accessed | tf_op | source)
XLA Modules:
  0.0 117.2 jit_solution(12462950090497491838)
XLA Ops:
  0.0 116.2 %shard_map.154 = bf16[1,512,1024]{2,1,0:T(8,128)(2,1)S(1)} custom-call(bf16[1,512,1024]{2,1,0:T(8,128)(2,1)} %stream_in.1, f32[1,1024]{1,0:T(1,128)} %bitcast.6, bf16[64,1024]{1,0:T(8,128)(2,1)} %value_in.1, bf16[64,1024]{1,0:T(8,128)(2,1)} %gate_in.1, bf16[31,1024]{1,0:T(8,128)(2,1)} %taps_in.1, f32[1,1024]{1,0:T(1,128)} %bitcast.7, f32[1,1024]{1,0:T(1,128)} %bitcast.8, ...), custom_call_target="tpu_custom_call" | custom-call | tf_op jit(solution)/shard_map/pallas_call | solution.py:461
  116.2 1.0 copy.18
